TPU v7x, 512 devices: a whole 4x4x16 slice. The times are simulated.
512 devices in a mesh: ep: 32 (over z, core), tp: 16 (over y, x).
Axes of the slice: x: 4, y: 4, z: 16, core: 2. Of those that a mesh axis runs over, the one named last changes fastest.
Arguments:
- value_in: bfloat16 [32768, 1536], P('ep', 'tp'), may hold values from -6 to 6
- gate_in: bfloat16 [32768, 1536], P('ep', 'tp'), may hold values from -9 to 9
- conv_kernel: float32 [31, 1536], P(None, 'tp'), may hold values from -40 to 40
- norm_gain: float32 [1536], replicated, may hold values from 0.1 to 1.9
- norm_shift: float32 [1536], replicated, may hold values from -3 to 3
- out_weight: bfloat16 [1536, 2048], P(None, 'tp'), may hold values from -0.15625 to 0.15625
- expert_input: bfloat16 [6144, 2048], P('ep'), may hold values from -6 to 6
- expert_gain: float32 [2048], replicated, may hold values from 0.1 to 1.9
- route_ids: int32 [6144, 4], P('ep'), may hold values from 0 to 31, all different within a row; in each aligned block of 192 rows (0 to 191, 192 to 383, ...) at most 30 rows name the same one
- route_weights: float32 [6144, 4], P('ep'), may hold values from 0.2 to 1
- gate_weight: bfloat16 [32, 2048, 2048], P('ep', None, 'tp'), may hold values from -0.375 to 0.375
- up_weight: bfloat16 [32, 2048, 2048], P('ep', None, 'tp'), may hold values from -0.375 to 0.375
- down_weight: bfloat16 [32, 2048, 2048], P('ep', None, 'tp'), may hold values from -0.01953125 to 0.01953125
Outputs:
- mixed_out: bfloat16 [32768, 2048], P('ep', 'tp')
- routed_out: bfloat16 [6144, 2048], P('ep', 'tp')
Inputs may be any that keep to these rules, and one draw needn't show every extreme that they name: `route_ids`: each row names 4 different experts; among the rows of one index of ep (aligned blocks of 192 rows) no expert is named by more than 30 rows, and in some block one expert is named by exactly 30.
All inputs are finite; a program needn't handle non-finite values.
Results may differ from a plain program's by a relative error of at most 0.0071.
Values may be sent and summed in bfloat16 or wider, within the bound.
A program may use at most 64 MiB of HBM per device.

v0:
```python
import jax
import jax.numpy as jnp
from jax import lax
from jax.sharding import PartitionSpec as P


def shifted(block, axis, distance):
    devices = range(lax.axis_size(axis))
    route = [(i - distance, i) for i in devices if i - distance in devices]
    return lax.ppermute(block, axis, route)


def laid_out(pieces, dim):
    pieces = jnp.moveaxis(pieces, 0, dim)
    lengths = pieces.shape
    return pieces.reshape(*lengths[:dim], lengths[dim] * lengths[dim + 1], *lengths[dim + 2 :])


def sent_to_all(shard, axis):
    copies = jnp.broadcast_to(shard, (lax.axis_size(axis), *shard.shape))
    return lax.all_to_all(copies, axis, split_axis=0, concat_axis=0, tiled=True)


def gather_directly(shard, axis, dim):
    return laid_out(sent_to_all(shard, axis), dim)


def expert_tail(gate_pre, up_pre, down_weight):
    clamped = jnp.minimum(gate_pre, 7.0)
    upward = jnp.clip(up_pre, -7.0, 7.0)
    activation = ((upward + 1.0) * clamped * jax.nn.sigmoid(1.702 * clamped)).astype(jnp.bfloat16)
    weights = down_weight[0]
    summed = jnp.dot(
        lax.all_gather(activation, "tp", axis=1, tiled=True),
        weights,
        preferred_element_type=jnp.float32,
    )
    return summed.astype(jnp.bfloat16)


def finish(gate_pre, up_pre, down_weight, arrived_shape):
    outcome = expert_tail(gate_pre, up_pre, down_weight)
    outcome = outcome.reshape(arrived_shape[0], arrived_shape[1], outcome.shape[1])
    return lax.all_to_all(outcome, "ep", split_axis=0, concat_axis=0, tiled=True)


def body(
    value_in,
    gate_in,
    conv_kernel,
    norm_gain,
    norm_shift,
    out_weight,
    expert_input,
    expert_gain,
    route_ids,
    route_weights,
    gate_weight,
    up_weight,
    down_weight,
):
    gated_values = (
        value_in.astype(jnp.float32) * jax.nn.sigmoid(gate_in.astype(jnp.float32))
    ).astype(jnp.bfloat16)
    kernel_width = conv_kernel.shape[0]
    length_dev = gated_values.shape[0]
    before = shifted(gated_values[length_dev - (kernel_width - 1) :], "ep", 1)
    extended = jnp.concatenate([before, gated_values], 0).astype(jnp.float32)
    running = jnp.zeros(gated_values.shape, jnp.float32)
    for tap_index in range(kernel_width):
        running = (
            running + conv_kernel[tap_index][None, :] * extended[tap_index : tap_index + length_dev]
        )
    convolved = running.astype(jnp.bfloat16)
    gathered = lax.all_gather(convolved, "tp", axis=1, tiled=True).astype(jnp.float32)
    row_mean = jnp.mean(gathered, axis=1, keepdims=True)
    row_var = jnp.mean(jnp.square(gathered - row_mean), axis=1, keepdims=True)
    normed = (gathered - row_mean) * lax.rsqrt(row_var + 1e-05) * norm_gain[None, :] + norm_shift[
        None, :
    ]
    hidden = jax.nn.silu(normed).astype(jnp.bfloat16)
    mixed_out = jnp.dot(hidden, out_weight, preferred_element_type=jnp.float32).astype(jnp.bfloat16)
    experts = lax.axis_size("ep")
    row_count, model_width = expert_input.shape
    top_count = route_ids.shape[1]
    capacity = (5 * row_count * top_count + 4 * experts - 1) // (4 * experts)
    input_float = expert_input.astype(jnp.float32)
    feature_mean = jnp.mean(input_float, axis=1, keepdims=True)
    feature_var = jnp.mean(jnp.square(input_float - feature_mean), axis=1, keepdims=True)
    normed_rows = (
        (input_float - feature_mean) * lax.rsqrt(feature_var + 1e-05) * expert_gain[None, :]
    ).astype(jnp.bfloat16)
    expert_ids = route_ids.reshape(-1)
    onehot = (expert_ids[:, None] == jnp.arange(experts, dtype=jnp.int32)[None, :]).astype(
        jnp.int32
    )
    earlier = jnp.cumsum(onehot, axis=0) - onehot
    position = jnp.sum(earlier * onehot, axis=1)
    destination = expert_ids * capacity + position
    token_index = jnp.arange(expert_ids.shape[0], dtype=jnp.int32) // top_count
    slot_token = (
        jnp.full((experts * capacity,), row_count, jnp.int32).at[destination].set(token_index)
    )
    padded = jnp.concatenate([normed_rows, jnp.zeros((1, model_width), jnp.bfloat16)], 0)
    outgoing = padded[slot_token].reshape(experts, capacity, model_width)
    column_width = model_width // lax.axis_size("tp")
    columns = lax.dynamic_slice_in_dim(
        outgoing, lax.axis_index("tp") * column_width, column_width, 2
    )
    arrived = lax.all_to_all(columns, "ep", split_axis=0, concat_axis=0, tiled=True)
    slot_total = arrived.shape[0] * arrived.shape[1]
    portion = gather_directly(arrived, "tp", 2)
    flattened = portion.reshape(slot_total, portion.shape[2])
    gate_part = gate_weight[0]
    up_part = up_weight[0]
    gate_pre = jnp.dot(flattened, gate_part, preferred_element_type=jnp.float32)
    up_pre = jnp.dot(flattened, up_part, preferred_element_type=jnp.float32)
    results_home = finish(gate_pre, up_pre, down_weight, arrived.shape)
    picked = results_home.reshape(-1, results_home.shape[2])[destination]
    picked = picked.reshape(row_count, top_count, -1).astype(jnp.float32)
    routed_out = jnp.sum(picked * route_weights[:, :, None], axis=1).astype(jnp.bfloat16)
    return (mixed_out, routed_out)


def solution(mesh):
    return jax.shard_map(
        body,
        mesh=mesh,
        in_specs=(
            P("ep", "tp"),
            P("ep", "tp"),
            P(None, "tp"),
            P(),
            P(),
            P(None, "tp"),
            P("ep", None),
            P(),
            P("ep", None),
            P("ep", None),
            P("ep", None, "tp"),
            P("ep", None, "tp"),
            P("ep", None, "tp"),
        ),
        out_specs=(P("ep", "tp"), P("ep", "tp")),
        check_vma=False,
    )
```

profile of v0, /device:TPU:1, one launch (start us, length us, event | category | flops | bytes accessed | tf_op | source)
XLA Modules:
  0.0 262.5 jit_solution(9652889797607337225)
XLA Ops:
  7.2 0.0 copy-start
  7.2 0.0 all-gather.3.cloned.1.call-start
  7.2 1.2 multiply_convert_fusion
  8.4 0.1 slice.264
  8.5 4.9 %collective-permute-start = (bf16[30,96]{0,1:T(8,128)(2,1)S(1)}, bf16[30,96]{0,1:T(8,128)(2,1)S(1)}, u32[]{:S(2)}, u32[]{:S(2)}) collective-permute-start(bf16[30,96]{0,1:T(8,128)(2,1)S(1)} %slice.264), channel_id=1, source_target_pairs={{0,16},{16,32},{32,48},{48,64},{64,80},{80,96},{96,112},{112,128},... | collective-permute-start | bytes 17288 | tf_op jit(solution)/shard_map/ppermute | solution.py:10
  13.4 1.0 slice_bitcast_fusion.30
  14.4 1.0 slice_bitcast_fusion.29
  15.4 0.8 copy.28
  16.2 0.1 eq.29
  16.3 0.1 eq.25
  16.4 0.7 broadcast_multiply_fusion
  17.1 1.7 reduce-window.6
  18.9 0.3 slice_reduce_fusion
  19.2 0.1 copy.27
  19.3 0.1 mul.496
  19.4 1.3 convert_reduce_fusion.1
  20.7 1.5 fusion.21
  22.2 0.1 fusion.82
  22.4 1.5 fusion.23
  23.9 0.1 concatenate.7
  24.0 3.4 %scatter_custom_fusion = s32[960]{0:T(1024)S(1)} fusion(s32[768]{0:T(1024)S(1)} %fusion.87, s32[768]{0:T(1024)S(1)} %add_select_fusion, s32[]{:T(128)} %constant.28.clone.1), kind=kCustom, calls=%fused_computation.130 | custom fusion | bytes 3844 | tf_op jit(solution)/shard_map/scatter | solution.py:102
  27.4 0.0 collective-permute-done
  27.4 0.1 maximum_convert_fusion
  27.6 4.7 %fusion.49 = bf16[1024,96]{0,1:T(8,128)(2,1)} fusion(f32[1054,96]{0,1:T(8,128)S(1)} %maximum_convert_fusion, f32[96]{0:T(128)S(1)} %get-tuple-element.31, f32[96]{0:T(128)S(1)} %get-tuple-element.32, f32[96]{0:T(128)S(1)} %get-tuple-element.3, f32[96]{0:T(128)S(1)} %get-tuple-element.4, f32[96]{0:T(128)S(1)} %get-tuple-element.5, ...), kind=kLoop, calls=%fused_computation.43 | loop fusion | flops 6094848 | bytes 12398208 | tf_op jit(solution)/shard_map/convert_element_type | solution.py:74
  32.3 0.0 all-gather.3.cloned.1.call-update
  32.3 0.0 all-gather.5.cloned.1.call-start
  32.4 5.9 %gather_fusion = bf16[960,2048]{1,0:T(8,128)(2,1)} fusion(bf16[193,2048]{1,0:T(8,128)(2,1)S(1)} %concatenate.7, s32[1024]{0:T(1024)S(1)} %pad_clamp_fusion.1), kind=kCustom, calls=%fused_computation | custom fusion | bytes 7868160 | tf_op jit(solution)/shard_map/gather | solution.py:105
  38.3 5.0 %reshape.91 = bf16[32,30,2048]{2,1,0:T(8,128)(2,1)} reshape(bf16[960,2048]{1,0:T(8,128)(2,1)} %gather_fusion) | data formatting | bytes 7864320 | tf_op jit(solution)/shard_map/reshape | solution.py:105
  43.3 1.0 constant_dynamic-slice_fusion
  44.3 36.5 %all_to_all.15 = bf16[32,30,128]{2,1,0:T(8,128)(2,1)S(1)} all-to-all(bf16[32,30,128]{2,1,0:T(8,128)(2,1)S(1)} %constant_dynamic-slice_fusion), channel_id=1, replica_groups=mesh['ep'=32,'tp'=16] {'ep'}, dimensions={0} | all-to-all | bytes 491520 | tf_op jit(solution)/shard_map/all_to_all | solution.py:110
  80.8 0.1 copy.31
  80.9 0.8 broadcast_in_dim.8
  81.7 59.7 %all_to_all.16 = bf16[16,32,30,128]{3,1,2,0:T(8,128)(2,1)S(1)} all-to-all(bf16[16,32,30,128]{3,1,2,0:T(8,128)(2,1)S(1)} %broadcast_in_dim.8), channel_id=1, replica_groups=mesh['ep'=32,'tp'=16] {'tp'}, dimensions={0} | all-to-all | bytes 7864320 | tf_op jit(solution)/shard_map/all_to_all | solution.py:21
  141.3 2.5 copy.32
  143.9 0.0 copy-done
  143.9 0.0 copy-start.3
  143.9 1.2 fusion.24
  145.1 0.0 copy-done.3
  145.1 0.0 copy-start.2
  145.1 0.0 copy-start.4
  145.1 1.9 fusion.42
  147.0 0.0 all-gather.5.cloned.1.call-update
  147.0 0.0 copy-done.2
  147.0 0.1 copy.33
  147.2 0.0 all-gather.3.cloned.1.call-done
  147.2 0.0 copy-start.1
  147.2 2.6 convert_reduce_fusion
  149.8 0.2 copy-done.1
  150.0 0.0 copy-start.5
  150.0 0.0 copy-start.6
  150.0 0.9 fusion.2
  150.9 61.1 %all-gather.5.cloned.1.call-done = bf16[960,2048]{1,0:T(8,128)(2,1)} async-done(((bf16[960,128]{1,0:T(8,128)(2,1)}), bf16[960,2048]{1,0:T(8,128)(2,1)}) %all-gather.5.cloned.1.call-update) | async-done | bytes 3932176 | tf_op jit(solution)/shard_map/all_gather | solution.py:34
  212.1 0.0 copy-done.4
  212.1 3.3 %convolution_convert_fusion = bf16[960,128]{1,0:T(8,128)(2,1)S(1)} fusion(bf16[960,2048]{1,0:T(8,128)(2,1)} %all-gather.5.cloned.1.call-done, bf16[1,2048,128]{2,1,0:T(8,128)(2,1)S(1)} %copy-done.4), kind=kOutput, calls=%fused_computation.37 | convolution fusion | flops 503439360 | bytes 4702208 | tf_op jit(solution)/shard_map/dot_general | solution.py:33
  215.4 0.8 reshape.92
  216.1 14.4 %all-to-all-start.2 = ((bf16[32,30,128]{2,1,0:T(8,128)(2,1)}), bf16[32,30,128]{2,1,0:T(8,128)(2,1)S(1)}, u32[]{:S(2)}, u32[]{:S(2)}) async-start(bf16[32,30,128]{2,1,0:T(8,128)(2,1)} %reshape.92), calls=%async_computation.2 | async-start | bytes 524288 | tf_op jit(solution)/shard_map/all_to_all | solution.py:44
  230.5 0.0 copy-done.5
  230.5 0.0 copy-done.6
  230.5 0.0 copy-done.7
  230.5 5.2 %fusion.39 = bf16[1024,128]{1,0:T(8,128)(2,1)} fusion(bf16[1536,128]{1,0:T(8,128)(2,1)S(1)} %copy-done.5, bf16[1024,1536]{0,1:T(8,128)(2,1)} %all-gather.3.cloned.1.call-done, f32[1536]{0:T(1024)S(1)} %copy-done.6, f32[1536]{0:T(1024)S(1)} %copy-done.7, f32[1024]{0:T(1024)S(1)} %add_rsqrt_fusion, f32[1024]{0:T(1024)S(1)} %broadcast_multiply_fusion.1), kind=kOutput, calls=%fused_computation.35 | convolution fusion | flops 418512896 | bytes 3821568 | tf_op jit(solution)/shard_map/dot_general | solution.py:82
  235.7 17.1 %all-to-all-done.2 = bf16[32,30,128]{2,1,0:T(8,128)(2,1)S(1)} async-done(((bf16[32,30,128]{2,1,0:T(8,128)(2,1)}), bf16[32,30,128]{2,1,0:T(8,128)(2,1)S(1)}, u32[]{:S(2)}, u32[]{:S(2)}) %all-to-all-start.2) | async-done | bytes 245792 | tf_op jit(solution)/shard_map/all_to_all | solution.py:44
  252.8 0.1 reshape.93
  252.8 1.9 gather_fusion.1
  254.7 1.0 fusion.79
  (12 shorter events, 0.1 us)
Async XLA Ops:
  7.2 136.7 %copy-start = (bf16[1,2048,128]{2,1,0:T(8,128)(2,1)S(1)}, bf16[1,2048,128]{2,1,0:T(8,128)(2,1)}, u32[]{:S(2)}) copy-start(bf16[1,2048,128]{2,1,0:T(8,128)(2,1)} %param.23) | copy-start | bytes 1572868
  7.2 140.0 %all-gather.3.cloned.1.call-start = ((), (), s32[]{:S(2)}) async-start(), calls=%async_computation.3 | async-start | bytes 3342336 | tf_op jit(solution)/shard_map/all_gather | solution.py:75
  8.5 18.9 %collective-permute-start = (bf16[30,96]{0,1:T(8,128)(2,1)S(1)}, bf16[30,96]{0,1:T(8,128)(2,1)S(1)}, u32[]{:S(2)}, u32[]{:S(2)}) collective-permute-start(bf16[30,96]{0,1:T(8,128)(2,1)S(1)} %slice.264), channel_id=1, source_target_pairs={{0,16},{16,32},{32,48},{48,64},{64,80},{80,96},{96,112},{112,128},... | collective-permute-start | bytes 17288 | tf_op jit(solution)/shard_map/ppermute | solution.py:10
  32.3 179.8 %all-gather.5.cloned.1.call-start = ((), (), s32[]{:S(2)}) async-start(), calls=%async_computation.4 | async-start | bytes 4177920 | tf_op jit(solution)/shard_map/all_gather | solution.py:34
  143.9 1.2 copy-start.3
  145.1 1.9 copy-start.2
  145.1 67.0 %copy-start.4 = (bf16[1,2048,128]{2,1,0:T(8,128)(2,1)S(1)}, bf16[1,2048,128]{2,1,0:T(8,128)(2,1)}, u32[]{:S(2)}) copy-start(bf16[1,2048,128]{2,1,0:T(8,128)(2,1)} %param.25) | copy-start | bytes 1572868
  147.2 2.8 %copy-start.1 = (bf16[1024,1536]{0,1:T(8,128)(2,1)S(1)}, bf16[1024,1536]{0,1:T(8,128)(2,1)}, u32[]{:S(2)}) copy-start(bf16[1024,1536]{0,1:T(8,128)(2,1)} %all-gather.3.cloned.1.call-done) | copy-start | bytes 9437188
  150.0 80.5 %copy-start.5 = (bf16[1536,128]{1,0:T(8,128)(2,1)S(1)}, bf16[1536,128]{1,0:T(8,128)(2,1)}, u32[]{:S(2)}) copy-start(bf16[1536,128]{1,0:T(8,128)(2,1)} %param.18) | copy-start | bytes 1179652
  150.0 80.5 %copy-start.6 = (f32[1536]{0:T(1024)S(1)}, f32[1536]{0:T(1024)}, u32[]{:S(2)}) copy-start(f32[1536]{0:T(1024)} %param.17) | copy-start | bytes 18436
  150.0 80.5 %copy-start.7 = (f32[1536]{0:T(1024)S(1)}, f32[1536]{0:T(1024)}, u32[]{:S(2)}) copy-start(f32[1536]{0:T(1024)} %param.16) | copy-start | bytes 18436
  216.1 36.6 %all-to-all-start.2 = ((bf16[32,30,128]{2,1,0:T(8,128)(2,1)}), bf16[32,30,128]{2,1,0:T(8,128)(2,1)S(1)}, u32[]{:S(2)}, u32[]{:S(2)}) async-start(bf16[32,30,128]{2,1,0:T(8,128)(2,1)} %reshape.92), calls=%async_computation.2 | async-start | bytes 524288 | tf_op jit(solution)/shard_map/all_to_all | solution.py:44
Sparse Core Ops, SparseCore 0:
  32.4 92.4 all-gather.2
  147.1 64.8 all-gather.4
where the time goes:
time: 263 us
  blocking collectives  96.2 us (37%)
  waiting for transfers between devices  78.3 us (30%)
  local copies, waits for them, and re-layouts  25.4 us (10%)
  starting transfers between devices  19.4 us (7%)
  other arithmetic  17.5 us (7%)
  between operations  14.3 us (5%)
  matrix products  11.5 us (4%)
    all_gather x1, waiting for transfers between devices, expert_tail(): lax.all_gather(activation, 'tp', axis=1, tiled=True)  61.1 us
    all_to_all x1, blocking collectives, sent_to_all(): return lax.all_to_all(copies, axis, split_axis=0, concat_axis=0, tiled=True)  59.7 us
    all_to_all x1, blocking collectives, body(): lax.all_to_all(columns, 'ep', split_axis=0, concat_axis=0, tiled=True)  36.5 us
    all_to_all x1, waiting for transfers between devices, finish(): lax.all_to_all(outcome, 'ep', split_axis=0, concat_axis=0, tiled=True)  17.1 us
    all_to_all x1, starting transfers between devices, finish(): lax.all_to_all(outcome, 'ep', split_axis=0, concat_axis=0, tiled=True)  14.4 us
    gather x1, local copies, waits for them, and re-layouts, body(): outgoing = padded[slot_token].reshape(experts, capacity, model_width)  5.91 us
  transfers between devices with their start and end apart: 4, of which 2 were waited for; matrix products, arithmetic and copies ran while one was open for 16% of the time, Pallas kernels for 0%

commit v1 on v0

v1 whole, which is shorter than its diff:
```python
import functools
import jax
import jax.numpy as jnp
from jax import lax
from jax.experimental import pallas as pl
from jax.experimental.pallas import tpu as pltpu
from jax.sharding import PartitionSpec as P

MESH = pl.DeviceIdType.MESH
NX = 4
NY = 4
NTP = NX * NY
NEP = 32
SLOT = 32


class TpGather:
    def __init__(self, src, buf, send, recv, base, row0=0, rows=None):
        self.src, self.buf, self.send_sem, self.recv_sem, self.base = src, buf, send, recv, base
        self.row0 = row0
        self.rows = buf.shape[1] if rows is None else rows
        tp = lax.axis_index("tp")
        self.tp, self.y, self.x = tp, tp // NX, lax.rem(tp, NX)
        self.sent = []

    def at(self, dy, dx):
        return lax.rem(self.y + (dy + NY), NY) * NX + lax.rem(self.x + (dx + NX), NX)

    def rel(self, h, first, second):
        return self.at(second, first) if h == 0 else self.at(first, second)

    def span(self, h, part):
        half = self.rows // 2
        if part is None:
            return pl.ds(self.row0 + h * half, half)
        return pl.ds(self.row0 + h * half + part * (half // 2), half // 2)

    def sem(self, h, phase, k, n):
        return self.base + h * 20 + (n if phase == 0 else 4 + 4 * k + n)

    def push(self, h, phase, k, first, second, part, direction):
        n = (0 if direction > 0 else 1) + (0 if part is None else 2)
        own = first == 0 and second == 0
        shard = self.rel(h, first, second)
        span = self.span(h, part)
        source = self.src.at[span] if own else self.buf.at[shard, span]
        to = self.rel(h, direction, 0) if phase == 0 else self.rel(h, 0, direction)
        i = self.sem(h, phase, k, n)
        copy = pltpu.make_async_remote_copy(
            src_ref=source,
            dst_ref=self.buf.at[shard, span],
            send_sem=self.send_sem.at[i],
            recv_sem=self.recv_sem.at[i],
            device_id={"tp": to},
            device_id_type=MESH,
        )
        copy.start()
        self.sent.append(copy)

    def arrive(self, h, phase, k, n):
        off = (-1, 1, 2, 2)[n]
        part = None if n < 2 else n - 2
        first = (0, -1, 1, 2)[k] if phase else off
        second = off if phase else 0
        span = self.span(h, part)
        place = self.buf.at[self.rel(h, first, second), span]
        i = self.sem(h, phase, k, n)
        pltpu.make_async_remote_copy(
            src_ref=place,
            dst_ref=place,
            send_sem=self.send_sem.at[i],
            recv_sem=self.recv_sem.at[i],
            device_id={"tp": self.at(0, 1)},
            device_id_type=MESH,
        ).wait_recv()

    def both(self, h, phase, k, first):
        self.push(h, phase, k, first, 0, None, 1)
        self.push(h, phase, k, first, 0, None, -1)

    def relay(self, h, phase, k, n):
        self.arrive(h, phase, k, n)
        off = (-1, 1)[n]
        first = (0, -1, 1, 2)[k] if phase else off
        second = off if phase else 0
        self.push(h, phase, k, first, second, n, -off)

    def start(self):
        for h in (0, 1):
            self.both(h, 0, 0, 0)
        for h in (0, 1):
            self.both(h, 1, 0, 0)

    def stage(self, s):
        if s == 0:
            for n in (0, 1):
                for h in (0, 1):
                    self.relay(h, 0, 0, n)
            for k in (1, 2):
                for h in (0, 1):
                    self.both(h, 1, k, (0, -1, 1, 2)[k])
        elif s == 1:
            for n in (0, 1):
                for h in (0, 1):
                    self.relay(h, 1, 0, n)
            for h in (0, 1):
                self.arrive(h, 0, 0, 2)
                self.arrive(h, 0, 0, 3)
                self.both(h, 1, 3, 2)
        elif s == 2:
            for k in (1, 2):
                for n in (0, 1):
                    for h in (0, 1):
                        self.relay(h, 1, k, n)
        elif s == 3:
            for n in (0, 1):
                for h in (0, 1):
                    self.relay(h, 1, 3, n)
        elif s == 4:
            for k in range(4):
                for n in (2, 3):
                    for h in (0, 1):
                        self.arrive(h, 1, k, n)

    def finish(self):
        for copy in self.sent:
            copy.wait_send()


def greet_plane():
    barrier = pltpu.get_barrier_semaphore()
    tp = lax.axis_index("tp")
    y, x = tp // NX, lax.rem(tp, NX)
    for dy, dx in ((0, 1), (0, 3), (1, 0), (3, 0)):
        to = lax.rem(y + dy, NY) * NX + lax.rem(x + dx, NX)
        pl.semaphore_signal(barrier, inc=1, device_id={"tp": to}, device_id_type=MESH)
    pl.semaphore_wait(barrier, 4)


def gather_kernel(src, buf, send, recv):
    greet_plane()
    gather = TpGather(src, buf, send, recv, 0)
    gather.start()
    buf[gather.tp] = src[...]
    for s in range(5):
        gather.stage(s)
    gather.finish()


def tp_gather(shard, number):
    rows, cols = shard.shape
    return pl.pallas_call(
        gather_kernel,
        out_shape=jax.ShapeDtypeStruct((NTP, rows, cols), shard.dtype),
        in_specs=[pl.BlockSpec(memory_space=pltpu.VMEM)],
        out_specs=pl.BlockSpec(memory_space=pltpu.VMEM),
        scratch_shapes=[pltpu.SemaphoreType.DMA((40,)), pltpu.SemaphoreType.DMA((40,))],
        compiler_params=pltpu.CompilerParams(collective_id=number, has_side_effects=True),
        name="tp_gather",
    )(shard)


def exchange_kernel(src, dst, send, recv):
    barrier = pltpu.get_barrier_semaphore()
    me = lax.axis_index("ep")
    for d in range(1, NEP):
        pl.semaphore_signal(
            barrier, inc=1, device_id={"ep": lax.rem(me + d, NEP)}, device_id_type=MESH
        )
    pl.semaphore_wait(barrier, NEP - 1)
    sent = []
    for d in sorted(range(1, NEP), key=lambda d: -min(d, NEP - d)):
        to = lax.rem(me + d, NEP)
        copy = pltpu.make_async_remote_copy(
            src_ref=src.at[to],
            dst_ref=dst.at[me],
            send_sem=send.at[d],
            recv_sem=recv.at[d],
            device_id={"ep": to},
            device_id_type=MESH,
        )
        copy.start()
        sent.append(copy)
    dst[me] = src[me]
    for d in range(1, NEP):
        came = lax.rem(me + NEP - d, NEP)
        pltpu.make_async_remote_copy(
            src_ref=dst.at[came],
            dst_ref=dst.at[came],
            send_sem=send.at[d],
            recv_sem=recv.at[d],
            device_id={"ep": came},
            device_id_type=MESH,
        ).wait_recv()
    for copy in sent:
        copy.wait_send()


def ep_exchange(blocks, number):
    return pl.pallas_call(
        exchange_kernel,
        out_shape=jax.ShapeDtypeStruct(blocks.shape, blocks.dtype),
        in_specs=[pl.BlockSpec(memory_space=pltpu.VMEM)],
        out_specs=pl.BlockSpec(memory_space=pltpu.VMEM),
        scratch_shapes=[pltpu.SemaphoreType.DMA((NEP,)), pltpu.SemaphoreType.DMA((NEP,))],
        compiler_params=pltpu.CompilerParams(collective_id=number, has_side_effects=True),
        name="ep_exchange",
    )(blocks)


def body(
    value_in,
    gate_in,
    conv_kernel,
    norm_gain,
    norm_shift,
    out_weight,
    expert_input,
    expert_gain,
    route_ids,
    route_weights,
    gate_weight,
    up_weight,
    down_weight,
):
    f32, bf16 = jnp.float32, jnp.bfloat16
    rows, width = expert_input.shape
    cols = width // NTP
    tp = lax.axis_index("tp")
    experts = jnp.arange(NEP, dtype=jnp.int32)
    chosen = route_ids[:, :, None] == experts[None, None, :]
    onehot = jnp.any(chosen, axis=1)
    share = jnp.sum(jnp.where(chosen, route_weights[:, :, None], 0.0), axis=1)
    earlier = (jnp.arange(rows)[:, None] > jnp.arange(rows)[None, :]).astype(bf16)
    place = jnp.dot(earlier, onehot.astype(bf16), preferred_element_type=f32)
    place = jnp.where(onehot, place.astype(jnp.int32), -1)
    slots = jnp.arange(SLOT, dtype=jnp.int32)
    pick = (place.T[:, None, :] == slots[None, :, None]).astype(bf16).reshape(NEP * SLOT, rows)
    wide = expert_input.astype(f32)
    mean = jnp.mean(wide, axis=1, keepdims=True)
    var = jnp.mean(jnp.square(wide - mean), axis=1, keepdims=True)
    mine = lax.dynamic_slice_in_dim(expert_input, tp * cols, cols, 1).astype(f32)
    gain = lax.dynamic_slice_in_dim(expert_gain, tp * cols, cols, 0)
    normed = ((mine - mean) * lax.rsqrt(var + 1e-05) * gain[None, :]).astype(bf16)
    outgoing = jnp.dot(pick, normed, preferred_element_type=f32).astype(bf16)
    arrived = ep_exchange(outgoing.reshape(NEP, SLOT, cols), 0)
    gathered = tp_gather(arrived.reshape(NEP * SLOT, cols), 1)
    flat = jnp.transpose(gathered, (1, 0, 2)).reshape(NEP * SLOT, width)
    gate_pre = jnp.dot(flat, gate_weight[0], preferred_element_type=f32)
    up_pre = jnp.dot(flat, up_weight[0], preferred_element_type=f32)
    clamped = jnp.minimum(gate_pre, 7.0)
    upward = jnp.clip(up_pre, -7.0, 7.0)
    activation = ((upward + 1.0) * clamped * jax.nn.sigmoid(1.702 * clamped)).astype(bf16)
    acts = tp_gather(activation, 2)
    acts = jnp.transpose(acts, (1, 0, 2)).reshape(NEP * SLOT, width)
    outcome = jnp.dot(acts, down_weight[0], preferred_element_type=f32).astype(bf16)
    home = ep_exchange(outcome.reshape(NEP, SLOT, cols), 3).reshape(NEP * SLOT, cols)
    mix = jnp.where(place[:, :, None] == slots[None, None, :], share[:, :, None], 0.0)
    mix = mix.reshape(rows, NEP * SLOT)
    mix_hi = mix.astype(bf16)
    mix_lo = (mix - mix_hi.astype(f32)).astype(bf16)
    routed_out = (
        jnp.dot(mix_hi, home, preferred_element_type=f32)
        + jnp.dot(mix_lo, home, preferred_element_type=f32)
    ).astype(bf16)
    gated = (value_in.astype(f32) * jax.nn.sigmoid(gate_in.astype(f32))).astype(bf16)
    taps = conv_kernel.shape[0]
    length = gated.shape[0]
    n = lax.axis_size("ep")
    before = lax.ppermute(
        gated[length - (taps - 1) :], "ep", [(i, i + 1) for i in range(n - 1)]
    )
    extended = jnp.concatenate([before, gated], 0).astype(f32)
    running = jnp.zeros(gated.shape, f32)
    for j in range(taps):
        running = running + conv_kernel[j][None, :] * extended[j : j + length]
    convolved = jnp.pad(running.astype(bf16), ((0, 0), (0, 128 - gated.shape[1])))
    full = tp_gather(convolved, 4)[:, :, : gated.shape[1]]
    full = jnp.transpose(full, (1, 0, 2)).reshape(length, -1).astype(f32)
    row_mean = jnp.mean(full, axis=1, keepdims=True)
    row_var = jnp.mean(jnp.square(full - row_mean), axis=1, keepdims=True)
    scaled = (full - row_mean) * lax.rsqrt(row_var + 1e-05) * norm_gain[None, :] + norm_shift[None, :]
    hidden = jax.nn.silu(scaled).astype(bf16)
    mixed_out = jnp.dot(hidden, out_weight, preferred_element_type=f32).astype(bf16)
    return (mixed_out, routed_out)


def solution(mesh):
    return jax.shard_map(
        body,
        mesh=mesh,
        in_specs=(
            P("ep", "tp"),
            P("ep", "tp"),
            P(None, "tp"),
            P(),
            P(),
            P(None, "tp"),
            P("ep", None),
            P(),
            P("ep", None),
            P("ep", None),
            P("ep", None, "tp"),
            P("ep", None, "tp"),
            P("ep", None, "tp"),
        ),
        out_specs=(P("ep", "tp"), P("ep", "tp")),
        check_vma=False,
    )
```

time: 263 us -> 214 us (0.81)
  Pallas kernels: 0 us -> 141 us
  blocking collectives: 96.2 us -> 0 us
  waiting for transfers between devices: 78.3 us -> 0.01 us
  starting transfers between devices: 19.4 us -> 4.92 us
  between operations: 14.3 us -> 0.87 us
  matrix products: 11.5 us -> 16.8 us
  other arithmetic: 17.5 us -> 20.3 us
    pallas_call x0 -> x5, Pallas kernels: none -> 141 us  [the longest x3 86.8 us: tp_gather(): pl.pallas_call(gather_kernel, out_shape=jax.ShapeDtypeStruct((NTP, rows,...]
    all_to_all x2 -> x0, blocking collectives: 96.2 us -> none  [the longest x1 59.7 us: sent_to_all(): return lax.all_to_all(copies, axis, split_axis=0, concat_axis=0, tiled=True)]
    all_gather x2 -> x0, waiting for transfers between devices: 61.2 us -> none  [the longest x1 61.1 us: expert_tail(): lax.all_gather(activation, 'tp', axis=1, tiled=True)]
    all_to_all x1 -> x0, waiting for transfers between devices: 17.1 us -> none  [finish(): lax.all_to_all(outcome, 'ep', split_axis=0, concat_axis=0, tiled=True)]
    all_to_all x1 -> x0, starting transfers between devices: 14.4 us -> none  [finish(): lax.all_to_all(outcome, 'ep', split_axis=0, concat_axis=0, tiled=True)]
    transpose x1 -> x2, local copies, waits for them, and re-layouts: 2.53 us -> 13.1 us  [the longest x1 6.59 us: body(): flat = jnp.transpose(gathered, (1, 0, 2)).reshape(NEP * SLOT, width)]
    convert_element_type x0 -> x2, local copies, waits for them, and re-layouts: none -> 9.65 us  [the longest x1 8.59 us: body(): full = jnp.transpose(full, (1, 0, 2)).reshape(length, -1).astype(f32)]
    gather x2 -> x0, local copies, waits for them, and re-layouts: 7.79 us -> none  [the longest x1 5.91 us: body(): outgoing = padded[slot_token].reshape(experts, capacity, model_width)]
  transfers between devices with their start and end apart: 4 -> 1, of which waited for: 2 -> 0; matrix products, arithmetic and copies ran while one was open for 16% -> 17% of each run, Pallas kernels for 0% -> 53%
where the time goes in v1:
time: 214 us; the launch traced here: 212 us
  Pallas kernels  141 us (66%)
  local copies, waits for them, and re-layouts  27.7 us (13%)
  other arithmetic  20.3 us (9%)
  matrix products  16.8 us (8%)
  starting transfers between devices  4.92 us (2%)
    pallas_call x3, Pallas kernels, tp_gather(): pl.pallas_call(gather_kernel, out_shape=jax.ShapeDtypeStruct((NTP, rows,...  86.8 us
    pallas_call x2, Pallas kernels, ep_exchange(): pl.pallas_call(exchange_kernel, out_shape=jax.ShapeDtypeStruct(blocks.sha...  54.7 us
    convert_element_type x1, local copies, waits for them, and re-layouts, body(): full = jnp.transpose(full, (1, 0, 2)).reshape(length, -1).astype(f32)  8.59 us
    transpose x1, local copies, waits for them, and re-layouts, body(): flat = jnp.transpose(gathered, (1, 0, 2)).reshape(NEP * SLOT, width)  6.59 us
    transpose x1, local copies, waits for them, and re-layouts, body(): acts = jnp.transpose(acts, (1, 0, 2)).reshape(NEP * SLOT, width)  6.47 us
    ppermute x1, starting transfers between devices, body(): lax.ppermute(gated[length - (taps - 1):], 'ep', [(i, i + 1) for i in rang...  4.92 us
  transfers between devices with their start and end apart: 1, of which 0 were waited for; matrix products, arithmetic and copies ran while one was open for 17% of the time, Pallas kernels for 53%

profile of v1, /device:TPU:1, one launch (start us, length us, event | category | flops | bytes accessed | tf_op | source)
XLA Modules:
  0.0 212.0 jit_solution(8495062391086602230)
XLA Ops:
  0.6 0.0 copy-start
  0.6 1.2 copy.31
  1.8 1.1 copy.32
  2.9 0.1 multiply_convert_fusion.1
  3.0 4.9 %collective-permute-start = (bf16[30,96]{1,0:T(8,128)(2,1)S(1)}, bf16[30,96]{1,0:T(8,128)(2,1)S(1)}, u32[]{:S(2)}, u32[]{:S(2)}) collective-permute-start(bf16[30,96]{1,0:T(8,128)(2,1)S(1)} %slice.256), channel_id=1, source_target_pairs={{0,16},{16,32},{32,48},{48,64},{64,80},{80,96},{96,112},{112,128},... | collective-permute-start | bytes 17288 | tf_op jit(solution)/shard_map/ppermute | solution.py:270
  8.0 1.3 convert_reduce_fusion.1
  9.3 1.5 fusion.6
  10.8 0.7 fusion.56
  11.5 1.0 slice_bitcast_fusion.30
  12.5 0.1 eq.58
  12.6 0.2 fusion.13
  12.8 0.7 select_reduce_fusion
  13.5 0.8 dynamic_slice.7
  14.3 0.2 bitcast_compare_fusion
  14.5 1.9 convolution_convert_fusion
  16.4 29.9 %ep_exchange.2 = bf16[32,32,128]{2,1,0:T(8,128)(2,1)} custom-call(bf16[32,32,128]{2,1,0:T(8,128)(2,1)} %bitcast.116), custom_call_target="tpu_custom_call" | custom-call | tf_op jit(solution)/shard_map/ep_exchange/pallas_call | solution.py:200
  46.3 30.9 %tp_gather.4 = bf16[16,1024,128]{2,1,0:T(8,128)(2,1)} custom-call(bf16[1024,128]{1,0:T(8,128)(2,1)} %bitcast.115), custom_call_target="tpu_custom_call" | custom-call | tf_op jit(solution)/shard_map/tp_gather/pallas_call | solution.py:152
  77.2 6.6 %copy.34 = bf16[1024,16,128]{0,2,1:T(8,128)(2,1)} copy(bf16[1024,16,128]{2,0,1:T(8,128)(2,1)} %bitcast.110) | data formatting | bytes 8388608 | tf_op jit(solution)/shard_map/transpose | solution.py:248
  83.8 0.0 copy-start.2
  83.8 0.0 copy-start.5
  83.8 0.0 copy-done
  83.8 3.6 %convolution_minimum_fusion = f32[1024,128]{1,0:T(8,128)S(1)} fusion(bf16[1024,2048]{0,1:T(8,128)(2,1)} %bitcast.112, bf16[1,2048,128]{2,1,0:T(8,128)(2,1)S(1)} %copy-done), kind=kOutput, calls=%fused_computation.16 | convolution fusion | flops 537001984 | bytes 5242880 | tf_op jit(solution)/shard_map/dot_general | solution.py:249
  87.4 0.0 copy-done.2
  87.5 0.0 copy-done.5
  87.5 2.0 fusion.10.src
  89.5 27.5 %tp_gather.5 = bf16[16,1024,128]{2,1,0:T(8,128)(2,1)} custom-call(bf16[1024,128]{1,0:T(8,128)(2,1)} %fusion.10.src), custom_call_target="tpu_custom_call" | custom-call | tf_op jit(solution)/shard_map/tp_gather/pallas_call | solution.py:152
  117.0 0.0 copy-start.6
  117.0 6.5 %copy.35 = bf16[1024,16,128]{0,2,1:T(8,128)(2,1)} copy(bf16[1024,16,128]{2,0,1:T(8,128)(2,1)} %bitcast.111) | data formatting | bytes 8388608 | tf_op jit(solution)/shard_map/transpose | solution.py:255
  123.4 0.0 copy-done.6
  123.4 4.2 %convolution_convert_fusion.2 = bf16[1024,128]{1,0:T(8,128)(2,1)} fusion(bf16[1024,2048]{0,1:T(8,128)(2,1)} %bitcast.114, bf16[1,2048,128]{2,1,0:T(8,128)(2,1)S(1)} %copy-done.6), kind=kOutput, calls=%fused_computation.24 | convolution fusion | flops 537001984 | bytes 4980736 | tf_op jit(solution)/shard_map/dot_general | solution.py:256
  127.6 24.8 %ep_exchange.3 = bf16[32,32,128]{2,1,0:T(8,128)(2,1)} custom-call(bf16[32,32,128]{2,1,0:T(8,128)(2,1)} %bitcast.117), custom_call_target="tpu_custom_call" | custom-call | tf_op jit(solution)/shard_map/ep_exchange/pallas_call | solution.py:200
  152.4 1.3 convolution_bitcast_fusion
  153.7 1.9 fusion.12
  155.6 1.0 slice_bitcast_fusion.29
  156.6 0.0 collective-permute-done
  156.6 0.1 maximum_convert_fusion
  156.7 2.1 fusion.17
  158.8 0.8 pad.4.src
  159.5 28.4 %tp_gather.3 = bf16[16,1024,128]{2,1,0:T(8,128)(2,1)} custom-call(bf16[1024,128]{1,0:T(8,128)(2,1)} %pad.4.src), custom_call_target="tpu_custom_call" | custom-call | tf_op jit(solution)/shard_map/tp_gather/pallas_call | solution.py:152
  188.0 0.0 copy-start.1
  188.0 3.2 %convert_reduce_fusion = f32[1024]{0:T(1024)S(1)} fusion(bf16[16,1024,128]{2,1,0:T(8,128)(2,1)} %tp_gather.3), kind=kLoop, calls=%fused_computation.1 | loop fusion | flops 3144704 | bytes 3149824 | tf_op jit(solution)/shard_map/reduce_sum | solution.py:280
  191.2 0.2 copy-done.1
  191.4 4.1 %convert_bitcast_fusion = f32[1024,16,96]{2,0,1:T(8,128)} fusion(bf16[16,1024,128]{2,1,0:T(8,128)(2,1)S(1)} %copy-done.1), kind=kLoop, calls=%fused_computation.2 | loop fusion | flops 1572864 | bytes 9437184 | tf_op jit(solution)/shard_map/convert_element_type | solution.py:279
  195.5 1.9 fusion.1
  197.4 0.0 copy-start.3
  197.4 0.0 copy-start.4
  197.4 8.6 %copy.33 = f32[1024,16,96]{0,2,1:T(8,128)} copy(f32[1024,16,96]{2,0,1:T(8,128)} %convert_bitcast_fusion) | data formatting | bytes 12582912 | tf_op jit(solution)/shard_map/convert_element_type | solution.py:279
  206.0 0.0 copy-done.3
  206.0 0.0 copy-done.4
  206.0 0.0 copy-start.7
  206.0 4.2 %multiply_convert_fusion = bf16[1024,1536]{0,1:T(8,128)(2,1)S(1)} fusion(f32[1024,16,96]{0,2,1:T(8,128)} %copy.33, f32[1536]{0:T(1024)S(1)} %copy-done.3, f32[1536]{0:T(1024)S(1)} %copy-done.4, f32[1024]{0:T(1024)S(1)} %add_rsqrt_fusion, f32[1024]{0:T(1024)S(1)} %broadcast_multiply_fusion), kind=kLoop, calls=%fused_computation.9 | loop fusion | flops 14155776 | bytes 9457664 | tf_op jit(solution)/shard_map/convert_element_type | solution.py:283
  210.3 0.0 copy-done.7
  210.3 1.7 convolution_convert_fusion.1
  (6 shorter events, 0.0 us)
Async XLA Ops:
  0.6 83.2 %copy-start = (bf16[1,2048,128]{2,1,0:T(8,128)(2,1)S(1)}, bf16[1,2048,128]{2,1,0:T(8,128)(2,1)}, u32[]{:S(2)}) copy-start(bf16[1,2048,128]{2,1,0:T(8,128)(2,1)} %param.23) | copy-start | bytes 1572868
  3.0 153.5 %collective-permute-start = (bf16[30,96]{1,0:T(8,128)(2,1)S(1)}, bf16[30,96]{1,0:T(8,128)(2,1)S(1)}, u32[]{:S(2)}, u32[]{:S(2)}) collective-permute-start(bf16[30,96]{1,0:T(8,128)(2,1)S(1)} %slice.256), channel_id=1, source_target_pairs={{0,16},{16,32},{32,48},{48,64},{64,80},{80,96},{96,112},{112,128},... | collective-permute-start | bytes 17288 | tf_op jit(solution)/shard_map/ppermute | solution.py:270
  83.8 3.6 %copy-start.2 = (bf16[1024,16,128]{0,2,1:T(8,128)(2,1)S(1)}, bf16[1024,16,128]{0,2,1:T(8,128)(2,1)}, u32[]{:S(2)}) copy-start(bf16[1024,16,128]{0,2,1:T(8,128)(2,1)} %copy.34) | copy-start | bytes 12582916
  83.8 3.6 %copy-start.5 = (bf16[1,2048,128]{2,1,0:T(8,128)(2,1)S(1)}, bf16[1,2048,128]{2,1,0:T(8,128)(2,1)}, u32[]{:S(2)}) copy-start(bf16[1,2048,128]{2,1,0:T(8,128)(2,1)} %param.24) | copy-start | bytes 1572868
  117.0 6.5 %copy-start.6 = (bf16[1,2048,128]{2,1,0:T(8,128)(2,1)S(1)}, bf16[1,2048,128]{2,1,0:T(8,128)(2,1)}, u32[]{:S(2)}) copy-start(bf16[1,2048,128]{2,1,0:T(8,128)(2,1)} %param.25) | copy-start | bytes 1572868
  188.0 3.5 %copy-start.1 = (bf16[16,1024,128]{2,1,0:T(8,128)(2,1)S(1)}, bf16[16,1024,128]{2,1,0:T(8,128)(2,1)}, u32[]{:S(2)}) copy-start(bf16[16,1024,128]{2,1,0:T(8,128)(2,1)} %tp_gather.3) | copy-start | bytes 12582916
  197.4 8.6 %copy-start.3 = (f32[1536]{0:T(1024)S(1)}, f32[1536]{0:T(1024)}, u32[]{:S(2)}) copy-start(f32[1536]{0:T(1024)} %param.17) | copy-start | bytes 18436
  197.4 8.6 %copy-start.4 = (f32[1536]{0:T(1024)S(1)}, f32[1536]{0:T(1024)}, u32[]{:S(2)}) copy-start(f32[1536]{0:T(1024)} %param.16) | copy-start | bytes 18436
  206.0 4.3 %copy-start.7 = (bf16[1536,128]{1,0:T(8,128)(2,1)S(1)}, bf16[1536,128]{1,0:T(8,128)(2,1)}, u32[]{:S(2)}) copy-start(bf16[1536,128]{1,0:T(8,128)(2,1)} %param.18) | copy-start | bytes 1179652

commit v2 on v1

v2 whole, which is shorter than its diff:
```python
import jax
import jax.numpy as jnp
from jax import lax
from jax.experimental import pallas as pl
from jax.experimental.pallas import tpu as pltpu
from jax.sharding import PartitionSpec as P

MESH = pl.DeviceIdType.MESH
F32, BF16 = jnp.float32, jnp.bfloat16
NX = 4
NY = 4
NTP = NX * NY
NEP = 32
HALF = 16
OTHER = 14
TAPS = 31
OFFS = (0, -1, 1, 2)


def sigmoid(v):
    return 0.5 * jnp.tanh(0.5 * v) + 0.5


class TpGather:
    def __init__(self, buf, send, recv, base, axis):
        self.buf, self.send_sem, self.recv_sem, self.base, self.axis = buf, send, recv, base, axis
        self.size = buf.shape[1 + axis]
        tp = lax.axis_index("tp")
        self.tp, self.y, self.x = tp, tp // NX, lax.rem(tp, NX)
        self.sent = []

    def at(self, dy, dx):
        return lax.rem(self.y + (dy + NY), NY) * NX + lax.rem(self.x + (dx + NX), NX)

    def rel(self, h, first, second):
        return self.at(second, first) if h == 0 else self.at(first, second)

    def place(self, h, first, second, part):
        half = self.size // 2
        span = (
            pl.ds(h * half, half)
            if part is None
            else pl.ds(h * half + part * (half // 2), half // 2)
        )
        shard = self.rel(h, first, second)
        return self.buf.at[shard, span] if self.axis == 0 else self.buf.at[shard, :, span]

    def sem(self, h, phase, k, n):
        return self.base + h * 20 + (n if phase == 0 else 4 + 4 * k + n)

    def push(self, h, phase, k, first, second, part, direction):
        n = (0 if direction > 0 else 1) + (0 if part is None else 2)
        place = self.place(h, first, second, part)
        to = self.rel(h, direction, 0) if phase == 0 else self.rel(h, 0, direction)
        i = self.sem(h, phase, k, n)
        copy = pltpu.make_async_remote_copy(
            src_ref=place,
            dst_ref=place,
            send_sem=self.send_sem.at[i],
            recv_sem=self.recv_sem.at[i],
            device_id={"tp": to},
            device_id_type=MESH,
        )
        copy.start()
        self.sent.append(copy)

    def arrive(self, h, phase, k, n):
        off = (-1, 1, 2, 2)[n]
        part = None if n < 2 else n - 2
        first = OFFS[k] if phase else off
        second = off if phase else 0
        place = self.place(h, first, second, part)
        i = self.sem(h, phase, k, n)
        pltpu.make_async_remote_copy(
            src_ref=place,
            dst_ref=place,
            send_sem=self.send_sem.at[i],
            recv_sem=self.recv_sem.at[i],
            device_id={"tp": self.at(0, 1)},
            device_id_type=MESH,
        ).wait_recv()

    def both(self, h, phase, k, first):
        self.push(h, phase, k, first, 0, None, 1)
        self.push(h, phase, k, first, 0, None, -1)

    def relay(self, h, phase, k, n):
        self.arrive(h, phase, k, n)
        off = (-1, 1)[n]
        first = OFFS[k] if phase else off
        second = off if phase else 0
        self.push(h, phase, k, first, second, n, -off)

    def start(self):
        for h in (0, 1):
            self.both(h, 0, 0, 0)
        for h in (0, 1):
            self.both(h, 1, 0, 0)

    def stage(self, s):
        if s == 0:
            for n in (0, 1):
                for h in (0, 1):
                    self.relay(h, 0, 0, n)
            for k in (1, 2):
                for h in (0, 1):
                    self.both(h, 1, k, OFFS[k])
        elif s == 1:
            for n in (0, 1):
                for h in (0, 1):
                    self.relay(h, 1, 0, n)
            for h in (0, 1):
                self.arrive(h, 0, 0, 2)
                self.arrive(h, 0, 0, 3)
                self.both(h, 1, 3, 2)
        elif s == 2:
            for k in (1, 2):
                for n in (0, 1):
                    for h in (0, 1):
                        self.relay(h, 1, k, n)
        elif s == 3:
            for n in (0, 1):
                for h in (0, 1):
                    self.relay(h, 1, 3, n)
        else:
            for k in range(4):
                for n in (2, 3):
                    for h in (0, 1):
                        self.arrive(h, 1, k, n)

    def finish(self):
        for copy in self.sent:
            copy.wait_send()


class Exchange:
    def __init__(self, src, dst, send, recv, number):
        self.src, self.dst = src, dst
        self.send_sem, self.recv_sem = send.at[number], recv.at[number]
        self.me = lax.axis_index("ep")

    def block(self, ref, index):
        return ref.at[pl.ds(pl.multiple_of(index * HALF, HALF), HALF)]

    def start(self):
        me = self.me

        def one(d):
            to = lax.rem(me + d, NEP)
            pltpu.make_async_remote_copy(
                src_ref=self.block(self.src, to),
                dst_ref=self.block(self.dst, me),
                send_sem=self.send_sem,
                recv_sem=self.recv_sem,
                device_id={"ep": to},
                device_id_type=MESH,
            ).start()

        one(NEP // 2)

        def pair(i, carry):
            one(NEP // 2 - i)
            one(NEP // 2 + i)
            return carry

        lax.fori_loop(1, NEP // 2, pair, 0)
        own = pl.ds(pl.multiple_of(me * HALF, HALF), HALF)
        self.dst[own] = self.src[own]

    def all_of(self):
        span = pl.ds(0, (NEP - 1) * HALF)
        return pltpu.make_async_remote_copy(
            src_ref=self.src.at[span],
            dst_ref=self.dst.at[span],
            send_sem=self.send_sem,
            recv_sem=self.recv_sem,
            device_id={"ep": lax.rem(self.me + 1, NEP)},
            device_id_type=MESH,
        )

    def arrive(self):
        self.all_of().wait_recv()

    def finish(self):
        self.all_of().wait_send()


def iota(shape, dim):
    return lax.broadcasted_iota(jnp.int32, shape, dim)


def dot(a, b):
    return jnp.dot(a, b, preferred_element_type=F32)


def conv_span(ext, taps_ref, cg, tp, channels, start, length):
    def group(g, carry):
        rows = pl.ds(pl.multiple_of(g * 16, 16), 16)
        wide = ext[rows, pl.ds(start - 128, length + 128)]
        taps = taps_ref[rows, :]
        total = jnp.zeros((16, length), F32)
        for j in range(TAPS):
            shift = TAPS - 1 - j
            moved = wide if shift == 0 else pltpu.roll(wide, shift, 1)
            total = total + taps[:, j : j + 1] * moved[:, 128:]
        cg[tp, rows, pl.ds(start - 128, length)] = total.astype(BF16)
        return carry

    lax.fori_loop(0, channels // 16, group, 0)


def kernel(
    value_ref,
    gate_ref,
    taps_ref,
    gain_ref,
    shift_ref,
    rows_ref,
    row_gain_ref,
    ids_ref,
    shares_ref,
    ow_hbm,
    wg_hbm,
    wu_hbm,
    wd_hbm,
    mixed_ref,
    routed_ref,
    ext,
    tail,
    halo,
    cg,
    out0,
    out1,
    arr1,
    x0,
    x1,
    h0,
    h1,
    y0,
    y1,
    r0,
    r1,
    ow,
    wgu,
    wd,
    load_sem,
    send,
    recv,
    zsend,
    zrecv,
    halo_sem,
):
    ep, tp = lax.axis_index("ep"), lax.axis_index("tp")
    channels, length = value_ref.shape
    count, width = rows_ref.shape
    cols = width // NTP

    barrier = pltpu.get_barrier_semaphore()
    y, x = tp // NX, lax.rem(tp, NX)
    for dy, dx in ((0, 1), (0, 3), (1, 0), (3, 0)):
        to = lax.rem(y + dy, NY) * NX + lax.rem(x + dx, NX)
        pl.semaphore_signal(barrier, inc=1, device_id={"tp": to}, device_id_type=MESH)

    def greet(d, carry):
        pl.semaphore_signal(
            barrier, inc=1, device_id={"ep": lax.rem(ep + d, NEP)}, device_id_type=MESH
        )
        return carry

    lax.fori_loop(1, NEP, greet, 0)

    loads = [
        pltpu.make_async_copy(wg_hbm.at[0], wgu.at[:, pl.ds(0, cols)], load_sem.at[0]),
        pltpu.make_async_copy(wu_hbm.at[0], wgu.at[:, pl.ds(cols, cols)], load_sem.at[1]),
        pltpu.make_async_copy(wd_hbm.at[0], wd, load_sem.at[2]),
        pltpu.make_async_copy(ow_hbm, ow, load_sem.at[3]),
    ]
    for load in loads:
        load.start()

    expert = iota((NEP, count), 0)
    chosen = jnp.zeros((NEP, count), F32)
    share = jnp.zeros((NEP, count), F32)
    for k in range(ids_ref.shape[0]):
        here = ids_ref[k : k + 1, :] == expert
        chosen = jnp.where(here, 1.0, chosen)
        share = jnp.where(here, shares_ref[k : k + 1, :], share)
    earlier = (iota((count, count), 0) < iota((count, count), 1)).astype(F32).astype(BF16)
    place = jnp.where(chosen > 0.5, dot(chosen.astype(BF16), earlier), -1.0)
    place_b = place.astype(BF16)
    total = jnp.zeros((count, cols), F32)
    for t in range(NTP):
        total = total + rows_ref[:, t * cols : (t + 1) * cols].astype(F32)
    mean = jnp.sum(total, axis=1, keepdims=True) * (1.0 / width)
    total = jnp.zeros((count, cols), F32)
    for t in range(NTP):
        off = rows_ref[:, t * cols : (t + 1) * cols].astype(F32) - mean
        total = total + off * off
    var = jnp.sum(total, axis=1, keepdims=True) * (1.0 / width)
    mine = rows_ref[:, pl.ds(pl.multiple_of(tp * cols, cols), cols)].astype(F32)
    normed = ((mine - mean) * lax.rsqrt(var + 1e-05) * row_gain_ref[pl.ds(tp, 1), :]).astype(BF16)
    spread = (lax.shift_right_logical(iota((NEP * HALF, NEP), 0), 4) == iota((NEP * HALF, NEP), 1))
    spread = spread.astype(F32).astype(BF16)
    slot_of = dot(spread, place_b)
    slot = jnp.bitwise_and(iota((NEP * HALF, count), 0), HALF - 1).astype(F32)
    for c, out in enumerate((out0, out1)):
        pick = (slot_of == slot + float(HALF * c)).astype(F32).astype(BF16)
        out[...] = dot(pick, normed).astype(BF16)

    gated = (value_ref[...].astype(F32) * sigmoid(gate_ref[...].astype(F32))).astype(BF16)
    tail[...] = gated[:, length - 128 :]
    ext[:, pl.ds(128, length)] = gated.astype(F32)
    conv_span(ext, taps_ref, cg, tp, channels, 256, length - 128)

    pl.semaphore_wait(barrier, 4 + NEP - 1)
    halo_copy = pltpu.make_async_remote_copy(
        src_ref=tail,
        dst_ref=halo,
        send_sem=halo_sem.at[0],
        recv_sem=halo_sem.at[1],
        device_id={"ep": lax.rem(ep + 1, NEP)},
        device_id_type=MESH,
    )
    halo_copy.start()
    go0 = Exchange(out0, x0.at[tp], zsend, zrecv, 0)
    go1 = Exchange(out1, arr1, zsend, zrecv, 1)
    go0.start()
    go1.start()
    halo_copy.wait_recv()
    ext[:, pl.ds(0, 128)] = jnp.where(ep > 0, halo[...].astype(F32), 0.0)
    conv_span(ext, taps_ref, cg, tp, channels, 128, 128)

    gc = TpGather(cg, send, recv, 0, 1)
    gx0 = TpGather(x0, send, recv, 40, 0)
    gx1 = TpGather(x1, send, recv, 80, 0)
    gh0 = TpGather(h0, send, recv, 120, 0)
    gh1 = TpGather(h1, send, recv, 160, 0)

    def up(xs, hs):
        n = xs.shape[1] // 2
        for i in range(2):
            lhs = jnp.concatenate([xs[t, i * n : (i + 1) * n, :] for t in range(NTP)], axis=1)
            pre = dot(lhs, wgu[...])
            g = jnp.minimum(pre[:, :cols], 7.0)
            u = jnp.clip(pre[:, cols:], -7.0, 7.0)
            hs[tp, pl.ds(i * n, n)] = ((u + 1.0) * g * sigmoid(1.702 * g)).astype(BF16)

    def down(hs):
        n = hs.shape[1] // 2
        parts = []
        for i in range(2):
            lhs = jnp.concatenate([hs[t, i * n : (i + 1) * n, :] for t in range(NTP)], axis=1)
            parts.append(dot(lhs, wd[...]).astype(BF16))
        return jnp.concatenate(parts, axis=0)

    few = NEP * OTHER

    def squeeze(shape, dim):
        row = iota(shape, dim).astype(F32)
        source = jnp.floor((row + 0.5) * (1.0 / OTHER))
        return row + source * float(HALF - OTHER)

    gc.start()
    gc.stage(0)
    go0.arrive()
    gx0.start()
    gc.stage(1)
    gx0.stage(0)
    go1.arrive()
    shrink = (squeeze((few, NEP * HALF), 0) == iota((few, NEP * HALF), 1).astype(F32)).astype(F32)
    x1[tp] = dot(shrink.astype(BF16), arr1[...]).astype(BF16)
    gc.stage(2)
    gx1.start()
    gx0.stage(1)
    gc.stage(3)
    gx1.stage(0)
    gx0.stage(2)
    gx1.stage(1)
    gx0.stage(3)
    loads[0].wait()
    loads[1].wait()
    gx0.stage(4)
    up(x0, h0)
    gh0.start()
    gx1.stage(2)
    gh0.stage(0)
    gx1.stage(3)
    gx1.stage(4)
    up(x1, h1)
    gh1.start()
    gh0.stage(1)
    gh1.stage(0)
    gh0.stage(2)
    gh1.stage(1)
    gh0.stage(3)
    loads[2].wait()
    gh0.stage(4)
    y0[...] = down(h0)
    back0 = Exchange(y0, r0, zsend, zrecv, 2)
    back0.start()
    gh1.stage(2)
    gh1.stage(3)
    gh1.stage(4)
    grow = (squeeze((NEP * HALF, few), 1) == iota((NEP * HALF, few), 0).astype(F32)).astype(F32)
    y1[...] = dot(grow.astype(BF16), down(h1)).astype(BF16)
    back1 = Exchange(y1, r1, zsend, zrecv, 3)
    back1.start()

    gc.stage(4)
    gc.finish()
    loads[3].wait()
    step = 256
    whole = NTP * channels
    turned = jnp.concatenate(
        [ow[i * 128 : (i + 1) * 128, :].T for i in range(whole // 128)], axis=1
    )

    def positions(i, carry):
        lanes = pl.ds(pl.multiple_of(i * step, step), step)
        acc = jnp.zeros((channels, step), F32)
        for t in range(NTP):
            acc = acc + cg[t, :, lanes].astype(F32)
        row_mean = jnp.sum(acc, axis=0, keepdims=True) * (1.0 / whole)
        acc = jnp.zeros((channels, step), F32)
        for t in range(NTP):
            off = cg[t, :, lanes].astype(F32) - row_mean
            acc = acc + off * off
        row_var = jnp.sum(acc, axis=0, keepdims=True) * (1.0 / whole)
        scale = lax.rsqrt(row_var + 1e-05)
        for t in range(NTP):
            part = slice(t * channels, (t + 1) * channels)
            v = (cg[t, :, lanes].astype(F32) - row_mean) * scale
            v = 0.5 * (v * gain_ref[part, :] + shift_ref[part, :])
            cg[t, :, lanes] = (v * jnp.tanh(v) + v).astype(BF16)
        hidden = jnp.concatenate([cg[t, :, lanes] for t in range(NTP)], axis=0)
        mixed = dot(turned, hidden)
        mixed_ref[lanes, :] = mixed.T.astype(BF16)
        return carry

    lax.fori_loop(0, length // step, positions, 0)

    def turn(a):
        eye = (iota((count, count), 0) == iota((count, count), 1)).astype(F32).astype(BF16)
        return lax.dot_general(eye, a, (((1,), (1,)), ((), ())), preferred_element_type=F32).astype(BF16)

    share_hi = share.astype(BF16)
    share_lo = (share - share_hi.astype(F32)).astype(BF16)
    widen = (lax.shift_right_logical(iota((NEP, NEP * HALF), 1), 4) == iota((NEP, NEP * HALF), 0))
    widen = widen.astype(F32).astype(BF16)
    slot_at = dot(turn(place_b), widen)
    hi_at = dot(turn(share_hi), widen)
    lo_at = dot(turn(share_lo), widen)
    slot = jnp.bitwise_and(iota((count, NEP * HALF), 1), HALF - 1).astype(F32)
    result = jnp.zeros((count, cols), F32)
    for c, (back, r) in enumerate(((back0, r0), (back1, r1))):
        back.arrive()
        there = slot_at == slot + float(HALF * c)
        result = result + dot(jnp.where(there, hi_at, 0.0).astype(BF16), r[...])
        result = result + dot(jnp.where(there, lo_at, 0.0).astype(BF16), r[...])
    routed_ref[...] = result.astype(BF16)

    halo_copy.wait_send()
    for moved in (go0, go1, gx0, gx1, gh0, gh1, back0, back1):
        moved.finish()


def body(
    value_in,
    gate_in,
    conv_kernel,
    norm_gain,
    norm_shift,
    out_weight,
    expert_input,
    expert_gain,
    route_ids,
    route_weights,
    gate_weight,
    up_weight,
    down_weight,
):
    length, channels = value_in.shape
    count, width = expert_input.shape
    cols = width // NTP
    few = NEP * OTHER
    many = NEP * HALF
    vmem = pl.BlockSpec(memory_space=pltpu.VMEM)
    hbm = pl.BlockSpec(memory_space=pltpu.HBM)
    mixed_out, routed_out = pl.pallas_call(
        kernel,
        out_shape=(
            jax.ShapeDtypeStruct((length, out_weight.shape[1]), BF16),
            jax.ShapeDtypeStruct((count, cols), BF16),
        ),
        in_specs=[vmem] * 9 + [hbm] * 4,
        out_specs=(vmem, vmem),
        scratch_shapes=[
            pltpu.VMEM((channels, 128 + length), F32),
            pltpu.VMEM((channels, 128), BF16),
            pltpu.VMEM((channels, 128), BF16),
            pltpu.VMEM((NTP, channels, length), BF16),
            pltpu.VMEM((many, cols), BF16),
            pltpu.VMEM((many, cols), BF16),
            pltpu.VMEM((many, cols), BF16),
            pltpu.VMEM((NTP, many, cols), BF16),
            pltpu.VMEM((NTP, few, cols), BF16),
            pltpu.VMEM((NTP, many, cols), BF16),
            pltpu.VMEM((NTP, few, cols), BF16),
            pltpu.VMEM((many, cols), BF16),
            pltpu.VMEM((many, cols), BF16),
            pltpu.VMEM((many, cols), BF16),
            pltpu.VMEM((many, cols), BF16),
            pltpu.VMEM(out_weight.shape, BF16),
            pltpu.VMEM((width, 2 * cols), BF16),
            pltpu.VMEM((width, cols), BF16),
            pltpu.SemaphoreType.DMA((4,)),
            pltpu.SemaphoreType.DMA((200,)),
            pltpu.SemaphoreType.DMA((200,)),
            pltpu.SemaphoreType.DMA((4,)),
            pltpu.SemaphoreType.DMA((4,)),
            pltpu.SemaphoreType.DMA((2,)),
        ],
        compiler_params=pltpu.CompilerParams(
            collective_id=0, has_side_effects=True, vmem_limit_bytes=60 * 1024 * 1024
        ),
        name="whole",
    )(
        value_in.T,
        gate_in.T,
        conv_kernel.T,
        norm_gain.reshape(-1, 1),
        norm_shift.reshape(-1, 1),
        expert_input,
        expert_gain.reshape(NTP, cols),
        route_ids.T,
        route_weights.T,
        out_weight,
        gate_weight,
        up_weight,
        down_weight,
    )
    return (mixed_out, routed_out)


def solution(mesh):
    return jax.shard_map(
        body,
        mesh=mesh,
        in_specs=(
            P("ep", "tp"),
            P("ep", "tp"),
            P(None, "tp"),
            P(),
            P(),
            P(None, "tp"),
            P("ep", None),
            P(),
            P("ep", None),
            P("ep", None),
            P("ep", None, "tp"),
            P("ep", None, "tp"),
            P("ep", None, "tp"),
        ),
        out_specs=(P("ep", "tp"), P("ep", "tp")),
        check_vma=False,
    )
```

time: 214 us -> 109 us (0.51)
  Pallas kernels: 141 us -> 102 us
  local copies, waits for them, and re-layouts: 27.7 us -> 6.06 us
  other arithmetic: 20.3 us -> 0 us
  matrix products: 16.8 us -> 0 us
  starting transfers between devices: 4.92 us -> 0 us
    pallas_call x5 -> x1, Pallas kernels: 141 us -> 102 us  [body(): pl.pallas_call(kernel, out_shape=(jax.ShapeDtypeStruct((length, out_weigh...]
    dot_general x8 -> x0, matrix products: 16.8 us -> none  [the longest x1 4.19 us: body(): jnp.dot(acts, down_weight[0], preferred_element_type=f32).astype(bf16)]
    transpose x2 -> x0, local copies, waits for them, and re-layouts: 13.1 us -> none  [the longest x1 6.59 us: body(): flat = jnp.transpose(gathered, (1, 0, 2)).reshape(NEP * SLOT, width)]
    convert_element_type x5 -> x0, other arithmetic: 10.6 us -> none  [the longest x1 4.24 us: body(): hidden = jax.nn.silu(scaled).astype(bf16)]
    convert_element_type x2 -> x0, local copies, waits for them, and re-layouts: 9.65 us -> none  [the longest x1 8.59 us: body(): full = jnp.transpose(full, (1, 0, 2)).reshape(length, -1).astype(f32)]
    reduce_sum x5 -> x0, other arithmetic: 8.68 us -> none  [the longest x1 3.23 us: body(): row_mean = jnp.mean(full, axis=1, keepdims=True)]
    ppermute x1 -> x0, starting transfers between devices: 4.92 us -> none  [body(): lax.ppermute(gated[length - (taps - 1):], 'ep', [(i, i + 1) for i in rang...]
    unnamed x17 -> x9, local copies, waits for them, and re-layouts: 1.41 us -> 3.75 us
  transfers between devices with their start and end apart: 1 -> 0, of which waited for: 0 -> 0; matrix products, arithmetic and copies ran while one was open for 17% -> 0% of each run, Pallas kernels for 53% -> 0%
where the time goes in v2:
time: 109 us
  Pallas kernels  102 us (94%)
  local copies, waits for them, and re-layouts  6.06 us (6%)
    pallas_call x1, Pallas kernels, body(): pl.pallas_call(kernel, out_shape=(jax.ShapeDtypeStruct((length, out_weigh...  102 us
    unnamed x9, local copies, waits for them, and re-layouts  3.75 us

profile of v2, /device:TPU:1, one launch (start us, length us, event | category | flops | bytes accessed | tf_op | source)
XLA Modules:
  0.0 109.0 jit_solution(14706869356504775473)
XLA Ops:
  0.6 0.0 copy-start.1
  0.6 1.4 %copy.16 = f32[31,96]{0,1:T(8,128)} copy(f32[31,96]{1,0:T(8,128)} %param.15) | data formatting | bytes 23808 | tf_op args[2]
  2.1 0.0 copy-done.1
  2.1 0.0 copy-start.2
  2.1 1.2 %reshape.16.gain_ref = f32[1536,1]{1,0:T(8,128)} reshape(f32[1536]{0:T(1024)S(1)} %copy-done.1) | data formatting | bytes 12288 | tf_op jit(solution)/shard_map/reshape | solution.py:531
  3.2 0.0 copy-done.2
  3.2 1.2 %reshape.17.shift_ref = f32[1536,1]{1,0:T(8,128)} reshape(f32[1536]{0:T(1024)S(1)} %copy-done.2) | data formatting | bytes 12288 | tf_op jit(solution)/shard_map/reshape | solution.py:532
  4.4 102.3 %whole.1 = (bf16[1024,128]{1,0:T(8,128)(2,1)}, bf16[192,128]{1,0:T(8,128)(2,1)}) custom-call(bf16[96,1024]{1,0:T(8,128)(2,1)} %bitcast.7, bf16[96,1024]{1,0:T(8,128)(2,1)} %bitcast.8, f32[96,31]{1,0:T(8,128)} %bitcast.6, f32[1536,1]{1,0:T(8,128)} %reshape.16.gain_ref, f32[1536,1]{1,0:T(8,128)} %reshape.17.shift_ref, bf16[192,2048]{1,0:T(8,128)(2,1)} %rows_ref.1, ...), custom_call_target="tpu_custom_call" | custom-call | tf_op jit(solution)/shard_map/whole/pallas_call | solution.py:489
  106.7 0.0 copy-start
  106.7 1.7 %copy.21 = bf16[1024,128]{1,0:T(8,128)(2,1)} copy(bf16[1024,128]{1,0:T(8,128)(2,1)} %get-tuple-element.4) | data formatting | bytes 524288
  108.4 0.0 copy-done
  108.4 0.6 copy.22
Async XLA Ops:
  0.6 1.4 %copy-start.1 = (f32[1536]{0:T(1024)S(1)}, f32[1536]{0:T(1024)}, u32[]{:S(2)}) copy-start(f32[1536]{0:T(1024)} %param.16) | copy-start | bytes 18436
  2.1 1.2 %copy-start.2 = (f32[1536]{0:T(1024)S(1)}, f32[1536]{0:T(1024)}, u32[]{:S(2)}) copy-start(f32[1536]{0:T(1024)} %param.17) | copy-start | bytes 18436
  106.7 1.7 %copy-start = (bf16[192,128]{1,0:T(8,128)(2,1)S(1)}, bf16[192,128]{1,0:T(8,128)(2,1)}, u32[]{:S(2)}) copy-start(bf16[192,128]{1,0:T(8,128)(2,1)} %get-tuple-element.5) | copy-start | bytes 147460

commit v3 on v2

v3 whole, which is shorter than its diff:
```python
import jax
import jax.numpy as jnp
from jax import lax
from jax.experimental import pallas as pl
from jax.experimental.pallas import tpu as pltpu
from jax.sharding import PartitionSpec as P

MESH = pl.DeviceIdType.MESH
F32, BF16 = jnp.float32, jnp.bfloat16
NX = 4
NY = 4
NTP = NX * NY
NEP = 32
HALF = 16
OTHER = 14
TAPS = 31
UNROLL = 3
OFFS = (0, -1, 1, 2)

ORDER = (
    "c.S", "convB", "c.E00", "c.E01", "c.E10", "c.E11", "c.R000", "c.R001", "c.R100", "c.R101",
    "c.F0", "c.R010", "c.R011", "c.R110", "c.R111", "c.R020", "c.R021", "c.F1", "c.R120", "c.R121",
    "go0", "x.S", "c.R030", "c.R031", "c.R130", "c.R131", "x.E10", "x.E11", "x.E00", "x.E01",
    "x.R000", "x.R001", "x.R100", "x.R101", "go1", "y.S", "c.D", "projc0", "x.F1", "projc1",
    "x.R010", "x.R011", "x.R110", "x.R111", "x.R120", "x.R121", "x.R020", "x.R021", "x.F0", "y.E10",
    "y.E11", "y.E00", "y.E01", "y.R000", "y.R001", "y.R100", "y.R101", "x.R130", "x.R131", "x.R030",
    "x.R031", "y.F1", "y.R110", "y.R111", "y.R010", "y.R011", "y.R120", "y.R121", "y.R020", "y.R021",
    "y.F0", "x.D", "up0", "h.S", "y.R130", "y.R131", "y.R030", "y.R031", "h.E00", "h.E01",
    "h.E10", "h.E11", "h.R000", "h.R001", "h.R100", "h.R101", "y.D", "up1", "k.S", "h.F0",
    "h.R010", "h.R011", "h.R110", "h.R111", "h.R020", "h.R021", "h.F1", "h.R120", "h.R121", "k.E00",
    "k.E01", "k.E10", "k.E11", "k.R000", "k.R001", "k.R100", "k.R101", "h.R030", "h.R031", "h.R130",
    "h.R131", "k.F0", "k.R010", "k.R011", "k.R110", "k.R111", "k.R020", "k.R021", "k.F1", "k.R120",
    "k.R121", "h.D", "down0", "l.S", "k.R030", "k.R031", "k.R130", "k.R131", "l.E00", "l.E01",
    "l.E10", "l.E11", "l.R000", "l.R001", "l.R100", "l.R101", "k.D", "down1", "l.F0", "l.R010",
    "l.R011", "l.R110", "l.R111", "l.R020", "l.R021", "l.F1", "prep", "l.R120", "l.R121", "l.R030", "l.R031",
    "l.R130", "l.R131", "sum0", "l.D", "projl0", "projl1", "sum1",
)


def sigmoid(v):
    return 0.5 * jnp.tanh(0.5 * v) + 0.5


class TpGather:
    def __init__(self, buf, send, recv, number, axis):
        self.buf, self.axis = buf, axis
        self.height = buf.shape[0] // NTP
        self.size = self.height if axis == 0 else buf.shape[1]
        self.send_sem, self.recv_sem, self.base = send.at[number], recv, number * 23
        tp = lax.axis_index("tp")
        self.y, self.x = tp // NX, lax.rem(tp, NX)

    def at(self, dy, dx):
        return lax.rem(self.y + (dy + NY), NY) * NX + lax.rem(self.x + (dx + NX), NX)

    def rel(self, h, first, second):
        return self.at(second, first) if h == 0 else self.at(first, second)

    def place(self, h, first, second, part):
        half = self.size // 2
        start, size = (h * half, half) if part is None else (h * half + part * (half // 2), half // 2)
        row = self.rel(h, first, second) * self.height
        if self.axis == 0:
            return self.buf.at[pl.ds(pl.multiple_of(row + start, 16), size)]
        return self.buf.at[pl.ds(pl.multiple_of(row, 16), self.height), pl.ds(start, size)]

    def sem(self, h, phase, k, n):
        if phase == 0:
            return self.recv_sem.at[self.base + h * 11 + min(n, 2)]
        return self.recv_sem.at[self.base + (h * 11 + 3 + 2 * k + n if n < 2 else 22)]

    def wait(self, place, sem):
        pltpu.make_async_remote_copy(
            src_ref=place,
            dst_ref=place,
            send_sem=self.send_sem,
            recv_sem=sem,
            device_id={"tp": self.at(0, 1)},
            device_id_type=MESH,
        ).wait_recv()

    def push(self, h, phase, k, first, second, part, direction):
        n = (0 if direction > 0 else 1) + (0 if part is None else 2)
        place = self.place(h, first, second, part)
        to = self.rel(h, direction, 0) if phase == 0 else self.rel(h, 0, direction)
        pltpu.make_async_remote_copy(
            src_ref=place,
            dst_ref=place,
            send_sem=self.send_sem,
            recv_sem=self.sem(h, phase, k, n),
            device_id={"tp": to},
            device_id_type=MESH,
        ).start()

    def both(self, h, phase, k, first):
        self.push(h, phase, k, first, 0, None, 1)
        self.push(h, phase, k, first, 0, None, -1)

    def relay(self, h, phase, k, n):
        off = (-1, 1)[n]
        first = OFFS[k] if phase else off
        second = off if phase else 0
        self.wait(self.place(h, first, second, None), self.sem(h, phase, k, n))
        self.push(h, phase, k, first, second, n, -off)

    def start(self):
        for h in (0, 1):
            self.both(h, 0, 0, 0)
        for h in (0, 1):
            self.both(h, 1, 0, 0)

    def run(self, step):
        kind, index = step[0], [int(i) for i in step[1:]]
        if kind == "S":
            self.start()
        elif kind == "E":
            h, n = index
            self.relay(h, 0, 0, n)
            self.both(h, 1, n + 1, OFFS[n + 1])
        elif kind == "F":
            (h,) = index
            self.wait(self.place(h, 2, 0, None), self.sem(h, 0, 0, 2))
            self.both(h, 1, 3, 2)
        elif kind == "R":
            h, k, n = index
            self.relay(h, 1, k, n)
        else:
            self.wait(self.buf.at[pl.ds(0, 4 * self.height)], self.sem(0, 1, 0, 2))

    def finish(self):
        place = self.buf.at[pl.ds(0, (NTP - 1) * self.height)]
        pltpu.make_async_remote_copy(
            src_ref=place,
            dst_ref=place,
            send_sem=self.send_sem,
            recv_sem=self.sem(0, 1, 0, 2),
            device_id={"tp": self.at(0, 1)},
            device_id_type=MESH,
        ).wait_send()


class Exchange:
    def __init__(self, src, dst, send, recv, number):
        self.src, self.dst = src, dst
        self.send_sem, self.recv_sem = send.at[number], recv.at[number]
        self.me = lax.axis_index("ep")

    def block(self, ref, index):
        return ref.at[pl.ds(pl.multiple_of(index * HALF, HALF), HALF)]

    def start(self):
        me = self.me

        def one(d):
            to = lax.rem(me + d, NEP)
            pltpu.make_async_remote_copy(
                src_ref=self.block(self.src, to),
                dst_ref=self.block(self.dst, me),
                send_sem=self.send_sem,
                recv_sem=self.recv_sem,
                device_id={"ep": to},
                device_id_type=MESH,
            ).start()

        one(NEP // 2)

        def pair(i, carry):
            one(NEP // 2 - i)
            one(NEP // 2 + i)
            return carry

        lax.fori_loop(1, NEP // 2, pair, 0)
        own = pl.ds(pl.multiple_of(me * HALF, HALF), HALF)
        self.dst[own] = self.src[own]

    def all_of(self):
        span = pl.ds(0, (NEP - 1) * HALF)
        return pltpu.make_async_remote_copy(
            src_ref=self.src.at[span],
            dst_ref=self.dst.at[span],
            send_sem=self.send_sem,
            recv_sem=self.recv_sem,
            device_id={"ep": lax.rem(self.me + 1, NEP)},
            device_id_type=MESH,
        )

    def arrive(self):
        self.all_of().wait_recv()

    def finish(self):
        self.all_of().wait_send()


def iota(shape, dim):
    return lax.broadcasted_iota(jnp.int32, shape, dim)


def dot(a, b):
    return jnp.dot(a, b, preferred_element_type=F32)


def conv_span(ext, taps, cg, tp, channels, start, length):
    def group(g, carry):
        parts = []
        for u in range(2):
            rows = pl.ds(pl.multiple_of(g * 16, 16) + 8 * u, 8)
            wide = ext[rows, pl.ds(start - 128, length + 128)]
            tap = taps[rows, :]
            sums = [None] * 4
            for b in range(8):
                moved = pltpu.roll(wide, b, 1) if b else wide
                for a in range(4):
                    j = TAPS - 1 - (8 * a + b)
                    if j >= 0:
                        term = tap[:, j : j + 1] * moved
                        sums[a] = term if sums[a] is None else sums[a] + term
            total = sums[0]
            for a in range(1, 4):
                total = total + pltpu.roll(sums[a], 8 * a, 1)
            parts.append(total[:, 128:])
        own = pl.ds(pl.multiple_of(tp * channels + g * 16, 16), 16)
        cg[own, :] = jnp.concatenate(parts, axis=0).astype(BF16)
        return carry

    lax.fori_loop(0, channels // 16, group, 0, unroll=UNROLL)


def kernel(
    value_hbm,
    gate_hbm,
    taps_hbm,
    gain_hbm,
    shift_hbm,
    rows_hbm,
    row_gain_hbm,
    ids_hbm,
    shares_hbm,
    ow_hbm,
    wg_hbm,
    wu_hbm,
    wd_hbm,
    mixed_ref,
    routed_ref,
    value_ref,
    gate_ref,
    taps_ref,
    gain_ref,
    shift_ref,
    rows_ref,
    row_gain_ref,
    ids_ref,
    shares_ref,
    ext,
    taps,
    tap_pad,
    tail,
    halo,
    cg_late,
    cg,
    out0,
    out1,
    arr1,
    x0,
    x1,
    h0,
    h1,
    y0,
    y1,
    r0,
    r1,
    mix,
    ow,
    wgu,
    wd,
    load_sem,
    send,
    recv,
    zsend,
    zrecv,
    halo_sem,
):
    ep, tp = lax.axis_index("ep"), lax.axis_index("tp")
    channels, length = value_hbm.shape
    count, width = rows_hbm.shape
    cols = width // NTP

    barrier = pltpu.get_barrier_semaphore()
    y, x = tp // NX, lax.rem(tp, NX)
    for dy, dx in ((0, 1), (0, 3), (1, 0), (3, 0)):
        to = lax.rem(y + dy, NY) * NX + lax.rem(x + dx, NX)
        pl.semaphore_signal(barrier, inc=1, device_id={"tp": to}, device_id_type=MESH)

    def greet(d, carry):
        pl.semaphore_signal(
            barrier, inc=1, device_id={"ep": lax.rem(ep + d, NEP)}, device_id_type=MESH
        )
        return carry

    lax.fori_loop(1, NEP, greet, 0)

    pairs = (
        (ids_hbm, ids_ref),
        (shares_hbm, shares_ref),
        (rows_hbm, rows_ref),
        (row_gain_hbm, row_gain_ref),
        (value_hbm, value_ref),
        (gate_hbm, gate_ref),
        (taps_hbm, taps_ref),
        (gain_hbm, gain_ref),
        (shift_hbm, shift_ref),
        (ow_hbm, ow),
        (wg_hbm.at[0], wgu.at[:, pl.ds(0, cols)]),
        (wu_hbm.at[0], wgu.at[:, pl.ds(cols, cols)]),
        (wd_hbm.at[0], wd),
    )
    loads = [pltpu.make_async_copy(a, b, load_sem.at[i]) for i, (a, b) in enumerate(pairs)]
    for load in loads:
        load.start()
    for load in loads[:4]:
        load.wait()

    expert = iota((NEP, count), 0)
    chosen = jnp.zeros((NEP, count), F32)
    share = jnp.zeros((NEP, count), F32)
    for k in range(ids_ref.shape[0]):
        here = ids_ref[k : k + 1, :] == expert
        chosen = jnp.where(here, 1.0, chosen)
        share = jnp.where(here, shares_ref[k : k + 1, :], share)
    earlier = (iota((count, count), 0) < iota((count, count), 1)).astype(F32).astype(BF16)
    place = jnp.where(chosen > 0.5, dot(chosen.astype(BF16), earlier), -1.0)
    place_b = place.astype(BF16)
    total = jnp.zeros((count, cols), F32)
    for t in range(NTP):
        total = total + rows_ref[:, t * cols : (t + 1) * cols].astype(F32)
    mean = jnp.sum(total, axis=1, keepdims=True) * (1.0 / width)
    total = jnp.zeros((count, cols), F32)
    for t in range(NTP):
        off = rows_ref[:, t * cols : (t + 1) * cols].astype(F32) - mean
        total = total + off * off
    var = jnp.sum(total, axis=1, keepdims=True) * (1.0 / width)
    mine = rows_ref[:, pl.ds(pl.multiple_of(tp * cols, cols), cols)].astype(F32)
    normed = ((mine - mean) * lax.rsqrt(var + 1e-05) * row_gain_ref[pl.ds(tp, 1), :]).astype(BF16)
    spread = (lax.shift_right_logical(iota((NEP * HALF, NEP), 0), 4) == iota((NEP * HALF, NEP), 1))
    spread = spread.astype(F32).astype(BF16)
    slot_of = dot(spread, place_b)
    slot = jnp.bitwise_and(iota((NEP * HALF, count), 0), HALF - 1).astype(F32)
    for c, out in enumerate((out0, out1)):
        pick = (slot_of == slot + float(HALF * c)).astype(F32).astype(BF16)
        out[...] = dot(pick, normed).astype(BF16)

    for load in loads[4:7]:
        load.wait()
    gated = (value_ref[...].astype(F32) * sigmoid(gate_ref[...].astype(F32))).astype(BF16)
    tail[...] = gated[:, length - 128 :]
    ext[:, pl.ds(128, length)] = gated.astype(F32)
    tap_pad[pl.ds(0, TAPS), pl.ds(0, channels)] = taps_ref[...]
    taps[...] = tap_pad[...].T

    pl.semaphore_wait(barrier, 4 + NEP - 1)
    halo_copy = pltpu.make_async_remote_copy(
        src_ref=tail,
        dst_ref=halo,
        send_sem=halo_sem.at[0],
        recv_sem=halo_sem.at[1],
        device_id={"ep": lax.rem(ep + 1, NEP)},
        device_id_type=MESH,
    )
    halo_copy.start()
    go0 = Exchange(out0, x0.at[pl.ds(pl.multiple_of(tp * out0.shape[0], 16), out0.shape[0])], zsend, zrecv, 0)
    go1 = Exchange(out1, arr1, zsend, zrecv, 1)
    go0.start()
    go1.start()
    half = length // 2
    conv_span(ext, taps, cg, tp, channels, 128 + half, half)
    gathers = {
        name: TpGather(ref, send, recv, i, axis)
        for i, (name, ref, axis) in enumerate(
            (("c", cg, 1), ("l", cg_late, 1), ("x", x0, 0), ("y", x1, 0), ("h", h0, 0), ("k", h1, 0))
        )
    }
    back0 = Exchange(y0, r0, zsend, zrecv, 2)
    back1 = Exchange(y1, r1, zsend, zrecv, 3)

    def conv_late():
        halo_copy.wait_recv()
        ext[:, pl.ds(0, 128)] = jnp.where(ep > 0, halo[...].astype(F32), 0.0)
        conv_span(ext, taps, cg_late, tp, channels, 128, half)

    def wide_rows(ref, i):
        n = ref.shape[0] // NTP
        return jnp.concatenate(
            [ref[t * n + i * (n // 2) : t * n + (i + 1) * (n // 2), :] for t in range(NTP)], axis=1
        )

    def up(xs, hs):
        n = xs.shape[0] // NTP
        for i in range(2):
            pre = dot(wide_rows(xs, i), wgu[...])
            g = jnp.minimum(pre[:, :cols], 7.0)
            u = jnp.clip(pre[:, cols:], -7.0, 7.0)
            own = pl.ds(pl.multiple_of(tp * n + i * (n // 2), 16), n // 2)
            hs[own, :] = ((u + 1.0) * g * sigmoid(1.702 * g)).astype(BF16)

    def down(hs):
        parts = [dot(wide_rows(hs, i), wd[...]).astype(BF16) for i in range(2)]
        return jnp.concatenate(parts, axis=0)

    few = NEP * OTHER

    def squeeze(shape, dim):
        row = iota(shape, dim).astype(F32)
        source = jnp.floor((row + 0.5) * (1.0 / OTHER))
        return row + source * float(HALF - OTHER)

    def compact():
        go1.arrive()
        row, col = squeeze((few, NEP * HALF), 0), iota((few, NEP * HALF), 1).astype(F32)
        own = pl.ds(pl.multiple_of(tp * few, 16), few)
        x1[own, :] = dot((row == col).astype(F32).astype(BF16), arr1[...]).astype(BF16)

    def return_first():
        y0[...] = down(h0)
        back0.start()

    def return_second():
        row, col = iota((NEP * HALF, few), 0).astype(F32), squeeze((NEP * HALF, few), 1)
        y1[...] = dot((row == col).astype(F32).astype(BF16), down(h1)).astype(BF16)
        back1.start()

    whole = NTP * channels
    groups = whole // 128
    step = 256

    def project_ready():
        for load in loads[7:10]:
            load.wait()
        blank = jnp.zeros((16 - groups, 128), F32)
        gains = jnp.concatenate([gain_ref[...], blank], axis=0).T
        shifts = jnp.concatenate([shift_ref[...], blank], axis=0).T
        turned = jnp.concatenate([ow[i * 128 : (i + 1) * 128, :].T for i in range(groups)], axis=1)
        return gains, shifts, turned

    def project(buf, i, first, gains, shifts, turned):
        lanes = pl.ds(i * step, step)
        acc = jnp.zeros((128, step), F32)
        for t in range(groups):
            acc = acc + buf[t * 128 : (t + 1) * 128, lanes].astype(F32)
        row_mean = jnp.sum(acc, axis=0, keepdims=True) * (1.0 / whole)
        acc = jnp.zeros((128, step), F32)
        for t in range(groups):
            off = buf[t * 128 : (t + 1) * 128, lanes].astype(F32) - row_mean
            acc = acc + off * off
        row_var = jnp.sum(acc, axis=0, keepdims=True) * (1.0 / whole)
        scale = lax.rsqrt(row_var + 1e-05)
        for t in range(groups):
            v = (buf[t * 128 : (t + 1) * 128, lanes].astype(F32) - row_mean) * scale
            v = 0.5 * (v * gains[:, t : t + 1] + shifts[:, t : t + 1])
            buf[t * 128 : (t + 1) * 128, lanes] = (v * jnp.tanh(v) + v).astype(BF16)
        mixed = dot(turned, buf[:, lanes])
        mixed_ref[pl.ds(first + i * step, step), :] = mixed.T.astype(BF16)

    def turn(a):
        eye = (iota((count, count), 0) == iota((count, count), 1)).astype(F32).astype(BF16)
        return lax.dot_general(eye, a, (((1,), (1,)), ((), ())), preferred_element_type=F32).astype(BF16)

    def prepare():
        share_hi = share.astype(BF16)
        share_lo = (share - share_hi.astype(F32)).astype(BF16)
        shape = (NEP, NEP * HALF)
        widen = lax.shift_right_logical(iota(shape, 1), 4) == iota(shape, 0)
        widen = widen.astype(F32).astype(BF16)
        slot_at = dot(turn(place_b), widen)
        hi_at = dot(turn(share_hi), widen)
        lo_at = dot(turn(share_lo), widen)
        slot = jnp.bitwise_and(iota((count, NEP * HALF), 1), HALF - 1).astype(F32)
        for c in range(2):
            there = slot_at == slot + float(HALF * c)
            mix[2 * c] = jnp.where(there, hi_at, 0.0).astype(BF16)
            mix[2 * c + 1] = jnp.where(there, lo_at, 0.0).astype(BF16)

    def weigh(c, back, r):
        back.arrive()
        return dot(mix[2 * c], r[...]) + dot(mix[2 * c + 1], r[...])

    tables = None
    partial = None
    for step_name in ORDER:
        if "." in step_name:
            gathers[step_name[0]].run(step_name[2:])
        elif step_name == "convB":
            conv_late()
        elif step_name == "go0":
            go0.arrive()
        elif step_name == "go1":
            compact()
        elif step_name == "up0":
            loads[10].wait()
            loads[11].wait()
            up(x0, h0)
        elif step_name == "up1":
            up(x1, h1)
        elif step_name == "down0":
            loads[12].wait()
            return_first()
        elif step_name == "down1":
            return_second()
        elif step_name == "projc0":
            gathers["c"].finish()
            tables = project_ready()
            project(cg, 0, half, *tables)
        elif step_name == "projc1":
            project(cg, 1, half, *tables)
        elif step_name == "projl0":
            gathers["l"].finish()
            project(cg_late, 0, 0, *tables)
        elif step_name == "projl1":
            project(cg_late, 1, 0, *tables)
        elif step_name == "prep":
            prepare()
        elif step_name == "sum0":
            partial = weigh(0, back0, r0)
        else:
            routed_ref[...] = (partial + weigh(1, back1, r1)).astype(BF16)

    halo_copy.wait_send()
    for moved in (go0, go1, *(gathers[name] for name in "xyhk"), back0, back1):
        moved.finish()


def body(
    value_in,
    gate_in,
    conv_kernel,
    norm_gain,
    norm_shift,
    out_weight,
    expert_input,
    expert_gain,
    route_ids,
    route_weights,
    gate_weight,
    up_weight,
    down_weight,
):
    length, channels = value_in.shape
    count, width = expert_input.shape
    cols = width // NTP
    few = NEP * OTHER
    many = NEP * HALF
    vmem = pl.BlockSpec(memory_space=pltpu.VMEM)
    hbm = pl.BlockSpec(memory_space=pltpu.HBM)
    mixed_out, routed_out = pl.pallas_call(
        kernel,
        out_shape=(
            jax.ShapeDtypeStruct((length, out_weight.shape[1]), BF16),
            jax.ShapeDtypeStruct((count, cols), BF16),
        ),
        in_specs=[hbm] * 13,
        out_specs=(vmem, vmem),
        scratch_shapes=[
            pltpu.VMEM((channels, length), BF16),
            pltpu.VMEM((channels, length), BF16),
            pltpu.VMEM(conv_kernel.shape, F32),
            pltpu.VMEM((NTP * channels // 128, 128), F32),
            pltpu.VMEM((NTP * channels // 128, 128), F32),
            pltpu.VMEM((count, width), BF16),
            pltpu.VMEM((NTP, cols), F32),
            pltpu.VMEM(route_ids.shape[::-1], jnp.int32),
            pltpu.VMEM(route_ids.shape[::-1], F32),
            pltpu.VMEM((channels, 128 + length), F32),
            pltpu.VMEM((128, 32), F32),
            pltpu.VMEM((32, 128), F32),
            pltpu.VMEM((channels, 128), BF16),
            pltpu.VMEM((channels, 128), BF16),
            pltpu.VMEM((NTP * channels, length // 2), BF16),
            pltpu.VMEM((NTP * channels, length // 2), BF16),
            pltpu.VMEM((many, cols), BF16),
            pltpu.VMEM((many, cols), BF16),
            pltpu.VMEM((many, cols), BF16),
            pltpu.VMEM((NTP * many, cols), BF16),
            pltpu.VMEM((NTP * few, cols), BF16),
            pltpu.VMEM((NTP * many, cols), BF16),
            pltpu.VMEM((NTP * few, cols), BF16),
            pltpu.VMEM((many, cols), BF16),
            pltpu.VMEM((many, cols), BF16),
            pltpu.VMEM((many, cols), BF16),
            pltpu.VMEM((many, cols), BF16),
            pltpu.VMEM((4, count, many), BF16),
            pltpu.VMEM(out_weight.shape, BF16),
            pltpu.VMEM((width, 2 * cols), BF16),
            pltpu.VMEM((width, cols), BF16),
            pltpu.SemaphoreType.DMA((13,)),
            pltpu.SemaphoreType.DMA((6,)),
            pltpu.SemaphoreType.DMA((6 * 23,)),
            pltpu.SemaphoreType.DMA((4,)),
            pltpu.SemaphoreType.DMA((4,)),
            pltpu.SemaphoreType.DMA((2,)),
        ],
        compiler_params=pltpu.CompilerParams(
            collective_id=0, has_side_effects=True, vmem_limit_bytes=60 * 1024 * 1024
        ),
        name="whole",
    )(
        value_in.T,
        gate_in.T,
        conv_kernel,
        norm_gain.reshape(-1, 128),
        norm_shift.reshape(-1, 128),
        expert_input,
        expert_gain.reshape(NTP, cols),
        route_ids.T,
        route_weights.T,
        out_weight,
        gate_weight,
        up_weight,
        down_weight,
    )
    return (mixed_out, routed_out)


def solution(mesh):
    return jax.shard_map(
        body,
        mesh=mesh,
        in_specs=(
            P("ep", "tp"),
            P("ep", "tp"),
            P(None, "tp"),
            P(),
            P(),
            P(None, "tp"),
            P("ep", None),
            P(),
            P("ep", None),
            P("ep", None),
            P("ep", None, "tp"),
            P("ep", None, "tp"),
            P("ep", None, "tp"),
        ),
        out_specs=(P("ep", "tp"), P("ep", "tp")),
        check_vma=False,
    )
```

time: 109 us -> 95.5 us (0.88)
  the two profiles are of different devices: /device:TPU:1 before, /device:TPU:4 now
where the time goes in v3:
time: 95.5 us; the launch traced here: 95.3 us
  Pallas kernels  92.4 us (97%)
  local copies, waits for them, and re-layouts  2.31 us (2%)
    pallas_call x1, Pallas kernels, body(): pl.pallas_call(kernel, out_shape=(jax.ShapeDtypeStruct((length, out_weigh...  92.4 us
    unnamed x4, local copies, waits for them, and re-layouts  2.31 us

profile of v3, /device:TPU:4, one launch (start us, length us, event | category | flops | bytes accessed | tf_op | source)
XLA Modules:
  0.0 95.3 jit_solution(5688209635598023968)
XLA Ops:
  0.6 92.4 %whole.1 = (bf16[1024,128]{1,0:T(8,128)(2,1)}, bf16[192,128]{1,0:T(8,128)(2,1)}) custom-call(bf16[96,1024]{1,0:T(8,128)(2,1)} %bitcast.7, bf16[96,1024]{1,0:T(8,128)(2,1)} %bitcast.8, f32[31,96]{1,0:T(8,128)} %taps_hbm.1, f32[12,128]{1,0:T(8,128)} %bitcast.9, f32[12,128]{1,0:T(8,128)} %bitcast.10, bf16[192,2048]{1,0:T(8,128)(2,1)} %rows_hbm.1, ...), custom_call_target="tpu_custom_call" | custom-call | tf_op jit(solution)/shard_map/whole/pallas_call | solution.py:552
  93.0 0.0 copy-start
  93.0 1.7 %copy.17 = bf16[1024,128]{1,0:T(8,128)(2,1)} copy(bf16[1024,128]{1,0:T(8,128)(2,1)} %get-tuple-element.4) | data formatting | bytes 524288
  94.7 0.0 copy-done
  94.7 0.6 copy.18
Async XLA Ops:
  93.0 1.7 %copy-start = (bf16[192,128]{1,0:T(8,128)(2,1)S(1)}, bf16[192,128]{1,0:T(8,128)(2,1)}, u32[]{:S(2)}) copy-start(bf16[192,128]{1,0:T(8,128)(2,1)} %get-tuple-element.5) | copy-start | bytes 147460

commit v4 on v3

v4 whole, which is shorter than its diff:
```python
import jax
import jax.numpy as jnp
from jax import lax
from jax.experimental import pallas as pl
from jax.experimental.pallas import tpu as pltpu
from jax.sharding import PartitionSpec as P

MESH = pl.DeviceIdType.MESH
F32, BF16 = jnp.float32, jnp.bfloat16
NX = 4
NY = 4
NTP = NX * NY
NEP = 32
HALF = 16
OTHER = 14
SLOTS = HALF + OTHER
NEAR = 10
FAR = 22
FAR_ROWS = FAR * HALF
LATE_ROWS = 320
NEAR_SEND = 32
NEAR_ROWS = 304
TAPS = 31
UNROLL = 6
OFFS = (0, -1, 1, 2)

ORDER = (
    0, 900, 10, 11, 12, 13, 20, 21, 28, 29, 2, 22, 23, 30, 31, 24,
    25, 3, 32, 33, 902, 200, 901, 26, 27, 34, 35, 212, 213, 210, 211, 220,
    221, 903, 300, 228, 229, 1, 910, 230, 231, 203, 911, 222, 223, 224, 225, 232,
    233, 202, 310, 311, 312, 313, 328, 329, 320, 321, 234, 235, 226, 227, 302, 322,
    323, 330, 331, 324, 325, 303, 332, 333, 914, 201, 904, 400, 326, 327, 334, 335,
    410, 411, 412, 413, 906, 420, 421, 428, 429, 301, 905, 500, 402, 422, 423, 430,
    431, 424, 425, 403, 432, 433, 510, 511, 512, 513, 600, 520, 521, 528, 529, 426,
    427, 434, 435, 502, 522, 523, 530, 531, 524, 525, 503, 532, 533, 610, 611, 612,
    613, 620, 621, 628, 629, 401, 907, 100, 526, 527, 534, 535, 602, 622, 623, 630,
    631, 624, 625, 603, 632, 633, 110, 111, 112, 113, 120, 121, 128, 129, 501, 908,
    626, 627, 634, 635, 102, 122, 123, 130, 131, 124, 125, 103, 132, 133, 601, 909,
    126, 127, 134, 135, 915, 101, 912, 913, 916, 917,
)


def sigmoid(v):
    return 0.5 * jnp.tanh(0.5 * v) + 0.5


class TpGather:
    def __init__(self, buf, send, recv, number, axis):
        self.buf, self.axis = buf, axis
        self.height = buf.shape[0] // NTP
        self.size = self.height if axis == 0 else buf.shape[1]
        self.send_sem, self.recv_sem, self.base = send.at[number], recv, number * 23
        unit = 16 if axis == 0 else 128
        whole = self.size // unit
        self.spans = {}
        for h, (at, size) in enumerate(((0, (whole + 1) // 2), ((whole + 1) // 2, whole // 2))):
            first = (size + 1) // 2
            self.spans[h, None] = (at * unit, size * unit)
            self.spans[h, 0] = (at * unit, first * unit)
            self.spans[h, 1] = ((at + first) * unit, (size - first) * unit)
        tp = lax.axis_index("tp")
        self.y, self.x = tp // NX, lax.rem(tp, NX)

    def at(self, dy, dx):
        return lax.rem(self.y + (dy + NY), NY) * NX + lax.rem(self.x + (dx + NX), NX)

    def rel(self, h, first, second):
        return self.at(second, first) if h == 0 else self.at(first, second)

    def place(self, h, first, second, part):
        start, size = self.spans[h, part]
        row = self.rel(h, first, second) * self.height
        if self.axis == 0:
            return self.buf.at[pl.ds(pl.multiple_of(row + start, 16), size)]
        return self.buf.at[pl.ds(pl.multiple_of(row, 16), self.height), pl.ds(start, size)]

    def sem(self, h, phase, k, n):
        if phase == 0:
            return self.recv_sem.at[self.base + h * 11 + min(n, 2)]
        return self.recv_sem.at[self.base + (h * 11 + 3 + 2 * k + n if n < 2 else 22)]

    def wait(self, place, sem):
        pltpu.make_async_remote_copy(
            src_ref=place,
            dst_ref=place,
            send_sem=self.send_sem,
            recv_sem=sem,
            device_id={"tp": self.at(0, 1)},
            device_id_type=MESH,
        ).wait_recv()

    def push(self, h, phase, k, first, second, part, direction):
        n = (0 if direction > 0 else 1) + (0 if part is None else 2)
        place = self.place(h, first, second, part)
        to = self.rel(h, direction, 0) if phase == 0 else self.rel(h, 0, direction)
        pltpu.make_async_remote_copy(
            src_ref=place,
            dst_ref=place,
            send_sem=self.send_sem,
            recv_sem=self.sem(h, phase, k, n),
            device_id={"tp": to},
            device_id_type=MESH,
        ).start()

    def both(self, h, phase, k, first):
        self.push(h, phase, k, first, 0, None, 1)
        self.push(h, phase, k, first, 0, None, -1)

    def relay(self, h, phase, k, n):
        off = (-1, 1)[n]
        first = OFFS[k] if phase else off
        second = off if phase else 0
        self.wait(self.place(h, first, second, None), self.sem(h, phase, k, n))
        self.push(h, phase, k, first, second, n, -off)

    def start(self):
        for h in (0, 1):
            self.both(h, 0, 0, 0)
        for h in (0, 1):
            self.both(h, 1, 0, 0)

    def run(self, step):
        if step == 0:
            self.start()
        elif step == 1:
            self.wait(self.buf.at[pl.ds(0, 4 * self.height)], self.sem(0, 1, 0, 2))
        elif step < 10:
            h = step - 2
            self.wait(self.place(h, 2, 0, None), self.sem(h, 0, 0, 2))
            self.both(h, 1, 3, 2)
        elif step < 20:
            h, n = (step - 10) // 2, step % 2
            self.relay(h, 0, 0, n)
            self.both(h, 1, n + 1, OFFS[n + 1])
        else:
            h, k, n = (step - 20) // 8, (step - 20) % 8 // 2, step % 2
            self.relay(h, 1, k, n)

    def finish(self):
        place = self.buf.at[pl.ds(0, (NTP - 1) * self.height)]
        pltpu.make_async_remote_copy(
            src_ref=place,
            dst_ref=place,
            send_sem=self.send_sem,
            recv_sem=self.sem(0, 1, 0, 2),
            device_id={"tp": self.at(0, 1)},
            device_id_type=MESH,
        ).wait_send()


class Exchange:
    def __init__(self, src, dst, send, recv, number, near):
        self.src, self.dst, self.near = src, dst, near
        self.send_sem, self.recv_sem = send.at[number], recv.at[number]
        self.me = lax.axis_index("ep")
        self.core = lax.rem(self.me, 2)
        self.rows = NEAR_SEND if near else HALF

    def block(self, ref, index):
        return ref.at[pl.ds(pl.multiple_of(index * self.rows, self.rows), self.rows)]

    def send(self, index, to, there):
        pltpu.make_async_remote_copy(
            src_ref=self.block(self.src, index),
            dst_ref=self.block(self.dst, there),
            send_sem=self.send_sem,
            recv_sem=self.recv_sem,
            device_id={"ep": to},
            device_id_type=MESH,
        ).start()

    def start(self):
        me, core = self.me, self.core
        if self.near:
            for j in (0, 1, 8, 9, 2, 3, 6, 7):
                self.send(j, lax.rem(me - core + (j - 4 + NEP), NEP), core + (8 - 2 * (j // 2)))
            self.send(5 - core, me + 1 - 2 * core, core + 4)
            own = pl.ds(pl.multiple_of((core + 4) * self.rows, self.rows), self.rows)
            self.dst[own, :] = self.src[own, :]
        else:
            for j in sorted(range(FAR), key=lambda j: abs(j // 2 - 5)):
                self.send(j, lax.rem(me - core + (j + 6), NEP), core + (20 - 2 * (j // 2)))

    def all_of(self):
        span = pl.ds(0, (NEAR - 1 if self.near else FAR) * self.rows)
        return pltpu.make_async_remote_copy(
            src_ref=self.src.at[span],
            dst_ref=self.dst.at[span],
            send_sem=self.send_sem,
            recv_sem=self.recv_sem,
            device_id={"ep": lax.rem(self.me + 1, NEP)},
            device_id_type=MESH,
        )

    def arrive(self):
        self.all_of().wait_recv()

    def finish(self):
        self.all_of().wait_send()


def iota(shape, dim):
    return lax.broadcasted_iota(jnp.int32, shape, dim)


def dot(a, b):
    return jnp.dot(a, b, preferred_element_type=F32)


def conv_span(ext, taps, cg, tp, channels, start, length):
    def group(g, carry):
        parts = []
        for u in range(2):
            rows = pl.ds(pl.multiple_of(g * 16, 16) + 8 * u, 8)
            wide = ext[rows, pl.ds(start - 128, length + 128)]
            tap = taps[rows, :]
            sums = [None] * 4
            for b in range(8):
                moved = pltpu.roll(wide, b, 1) if b else wide
                for a in range(4):
                    j = TAPS - 1 - (8 * a + b)
                    if j >= 0:
                        lane = jnp.broadcast_to(tap[:, j : j + 1], (8, 128))
                        term = jnp.concatenate([lane] * (length // 128 + 1), axis=1) * moved
                        sums[a] = term if sums[a] is None else sums[a] + term
            total = sums[0]
            for a in range(1, 4):
                total = total + pltpu.roll(sums[a], 8 * a, 1)
            parts.append(total[:, 128:])
        own = pl.ds(pl.multiple_of(tp * channels + g * 16, 16), 16)
        cg[own, :] = jnp.concatenate(parts, axis=0).astype(BF16)
        return carry

    lax.fori_loop(0, channels // 16, group, 0, unroll=UNROLL)


def kernel(
    value_hbm,
    gate_hbm,
    taps_hbm,
    gain_hbm,
    shift_hbm,
    rows_hbm,
    row_gain_hbm,
    ids_hbm,
    shares_hbm,
    ow_hbm,
    wg_hbm,
    wu_hbm,
    wd_hbm,
    mixed_ref,
    routed_ref,
    value_ref,
    gate_ref,
    taps_ref,
    gain_ref,
    shift_ref,
    rows_ref,
    row_gain_ref,
    ids_ref,
    shares_ref,
    ext,
    taps,
    tap_pad,
    tail,
    halo,
    cg_late,
    cg,
    out0,
    out1,
    outn,
    arr1,
    near,
    x0,
    x1,
    h0,
    h1,
    hn,
    y0,
    y1,
    yn,
    r0,
    r1,
    rn,
    mix,
    mixn,
    ow,
    wgu,
    wd,
    load_sem,
    send,
    recv,
    zsend,
    zrecv,
    halo_sem,
):
    ep, tp = lax.axis_index("ep"), lax.axis_index("tp")
    channels, length = value_hbm.shape
    count, width = rows_hbm.shape
    cols = width // NTP

    barrier = pltpu.get_barrier_semaphore()
    y, x = tp // NX, lax.rem(tp, NX)
    for dy, dx in ((0, 1), (0, 3), (1, 0), (3, 0)):
        to = lax.rem(y + dy, NY) * NX + lax.rem(x + dx, NX)
        pl.semaphore_signal(barrier, inc=1, device_id={"tp": to}, device_id_type=MESH)

    def greet(d, carry):
        pl.semaphore_signal(
            barrier, inc=1, device_id={"ep": lax.rem(ep + d, NEP)}, device_id_type=MESH
        )
        return carry

    lax.fori_loop(1, NEP, greet, 0)

    pairs = (
        (ids_hbm, ids_ref),
        (shares_hbm, shares_ref),
        (rows_hbm, rows_ref),
        (row_gain_hbm, row_gain_ref),
        (value_hbm, value_ref),
        (gate_hbm, gate_ref),
        (taps_hbm, taps_ref),
        (gain_hbm, gain_ref),
        (shift_hbm, shift_ref),
        (ow_hbm, ow),
        (wg_hbm.at[0], wgu.at[:, pl.ds(0, cols)]),
        (wu_hbm.at[0], wgu.at[:, pl.ds(cols, cols)]),
        (wd_hbm.at[0], wd),
    )
    loads = [pltpu.make_async_copy(a, b, load_sem.at[i]) for i, (a, b) in enumerate(pairs)]
    for load in loads:
        load.start()
    for load in loads[:2]:
        load.wait()

    expert = iota((NEP, count), 0)
    chosen = jnp.zeros((NEP, count), F32)
    share = jnp.zeros((NEP, count), F32)
    for k in range(ids_ref.shape[0]):
        here = ids_ref[k : k + 1, :] == expert
        chosen = jnp.where(here, 1.0, chosen)
        share = jnp.where(here, shares_ref[k : k + 1, :], share)
    earlier = (iota((count, count), 0) < iota((count, count), 1)).astype(F32).astype(BF16)
    place = jnp.where(chosen > 0.5, dot(chosen.astype(BF16), earlier), -1.0)
    place_b = place.astype(BF16)
    for load in loads[2:4]:
        load.wait()
    total = jnp.zeros((count, cols), F32)
    for t in range(NTP):
        total = total + rows_ref[:, t * cols : (t + 1) * cols].astype(F32)
    mean = jnp.sum(total, axis=1, keepdims=True) * (1.0 / width)
    total = jnp.zeros((count, cols), F32)
    for t in range(NTP):
        off = rows_ref[:, t * cols : (t + 1) * cols].astype(F32) - mean
        total = total + off * off
    var = jnp.sum(total, axis=1, keepdims=True) * (1.0 / width)
    mine = rows_ref[:, pl.ds(pl.multiple_of(tp * cols, cols), cols)].astype(F32)
    normed = ((mine - mean) * lax.rsqrt(var + 1e-05) * row_gain_ref[pl.ds(tp, 1), :]).astype(BF16)
    base = ep - lax.rem(ep, 2)

    def owners(shape, dim, bits, first):
        owner = jnp.bitwise_and(lax.shift_right_logical(iota(shape, dim), bits) + (base + first + NEP), NEP - 1)
        return (owner == iota(shape, 1 - dim)).astype(F32).astype(BF16)

    slot_of = dot(owners((FAR_ROWS, NEP), 0, 4, 6), place_b)
    slot = jnp.bitwise_and(iota((FAR_ROWS, count), 0), HALF - 1).astype(F32)
    for c, out in enumerate((out0, out1)):
        pick = (slot_of == slot + float(HALF * c)).astype(F32).astype(BF16)
        out[...] = dot(pick, normed).astype(BF16)

    def send_near():
        shape = (NEAR * NEAR_SEND, count)
        at = dot(owners((shape[0], NEP), 0, 5, -4), place_b)
        slot = jnp.bitwise_and(iota(shape, 0), NEAR_SEND - 1).astype(F32)
        pick = (at == slot).astype(F32).astype(BF16)
        scale = lax.rsqrt(var + 1e-05)
        for t in range(0, NTP, 2):
            parts = []
            for u in (t, t + 1):
                part = (rows_ref[:, u * cols : (u + 1) * cols].astype(F32) - mean) * scale
                parts.append((part * row_gain_ref[u : u + 1, :]).astype(BF16))
            pair = dot(pick, jnp.concatenate(parts, axis=1))
            outn[:, t * cols : (t + 2) * cols] = pair.astype(BF16)
        gon.start()

    for load in loads[4:7]:
        load.wait()
    gated = (value_ref[...].astype(F32) * sigmoid(gate_ref[...].astype(F32))).astype(BF16)
    tail[...] = gated[:, length - 128 :]
    ext[:, pl.ds(128, length)] = gated.astype(F32)
    tap_pad[pl.ds(0, TAPS), pl.ds(0, channels)] = taps_ref[...]
    taps[...] = tap_pad[...].T

    pl.semaphore_wait(barrier, 4 + NEP - 1)
    halo_copy = pltpu.make_async_remote_copy(
        src_ref=tail,
        dst_ref=halo,
        send_sem=halo_sem.at[0],
        recv_sem=halo_sem.at[1],
        device_id={"ep": lax.rem(ep + 1, NEP)},
        device_id_type=MESH,
    )
    halo_copy.start()
    own = pl.ds(pl.multiple_of(tp * FAR_ROWS, 16), FAR_ROWS)
    go0 = Exchange(out0, x0.at[own], zsend, zrecv, 0, False)
    go1 = Exchange(out1, arr1, zsend, zrecv, 1, False)
    gon = Exchange(outn, near, zsend, zrecv, 2, True)
    go0.start()
    go1.start()
    half = length // 2
    conv_span(ext, taps, cg, tp, channels, 128 + half, half)
    refs = ((cg, 1), (cg_late, 1), (x0, 0), (x1, 0), (h0, 0), (h1, 0), (hn, 0))
    gathers = [TpGather(ref, send, recv, i, axis) for i, (ref, axis) in enumerate(refs)]
    back0 = Exchange(y0, r0, zsend, zrecv, 3, False)
    back1 = Exchange(y1, r1, zsend, zrecv, 4, False)
    backn = Exchange(yn, rn, zsend, zrecv, 5, True)

    def conv_late():
        halo_copy.wait_recv()
        ext[:, pl.ds(0, 128)] = jnp.where(ep > 0, halo[...].astype(F32), 0.0)
        conv_span(ext, taps, cg_late, tp, channels, 128, half)

    def halves(n):
        first = (n // 16 + 1) // 2 * 16
        return (0, first), (first, n - first)

    def wide_rows(ref, start, size):
        n = ref.shape[0] // NTP
        return jnp.concatenate([ref[t * n + start : t * n + start + size, :] for t in range(NTP)], axis=1)

    def activate(lhs):
        pre = dot(lhs, wgu[...])
        g = jnp.minimum(pre[:, :cols], 7.0)
        u = jnp.clip(pre[:, cols:], -7.0, 7.0)
        return ((u + 1.0) * g * sigmoid(1.702 * g)).astype(BF16)

    def up(xs, hs):
        n = xs.shape[0] // NTP
        for start, size in halves(n):
            own = pl.ds(pl.multiple_of(tp * n + start, 16), size)
            hs[own, :] = activate(wide_rows(xs, start, size))

    def down(hs):
        parts = [dot(wide_rows(hs, *part), wd[...]).astype(BF16) for part in halves(hs.shape[0] // NTP)]
        return jnp.concatenate(parts, axis=0)

    def moved(shape, dim, block, room):
        row = iota(shape, dim).astype(F32)
        row = row + jnp.floor((row + 0.5) * (1.0 / block)) * float(room - block)
        return (row == iota(shape, 1 - dim).astype(F32)).astype(F32).astype(BF16)

    def compact():
        go1.arrive()
        own = pl.ds(pl.multiple_of(tp * LATE_ROWS, 16), LATE_ROWS)
        x1[own, :] = dot(moved((LATE_ROWS, FAR_ROWS), 0, OTHER, HALF), arr1[...]).astype(BF16)

    def up_near():
        gon.arrive()
        room = NEAR * NEAR_SEND
        act = [activate(near[i * room // 2 : (i + 1) * room // 2, :]) for i in range(2)]
        own = pl.ds(pl.multiple_of(tp * NEAR_ROWS, 16), NEAR_ROWS)
        turn_in = moved((NEAR_ROWS, room), 0, SLOTS, NEAR_SEND)
        hn[own, :] = dot(turn_in, jnp.concatenate(act, axis=0)).astype(BF16)

    def return_first():
        y0[...] = down(h0)
        back0.start()

    def return_second():
        y1[...] = dot(moved((FAR_ROWS, LATE_ROWS), 1, OTHER, HALF), down(h1)).astype(BF16)
        back1.start()

    def return_near():
        turn_out = moved((NEAR * NEAR_SEND, NEAR_ROWS), 1, SLOTS, NEAR_SEND)
        yn[...] = dot(turn_out, down(hn)).astype(BF16)
        backn.start()

    whole = NTP * channels
    groups = whole // 128
    stride = 256

    def project_ready():
        for load in loads[7:10]:
            load.wait()
        blank = jnp.zeros((16 - groups, 128), F32)
        gains = 0.5 * jnp.concatenate([gain_ref[...], blank], axis=0).T
        shifts = 0.5 * jnp.concatenate([shift_ref[...], blank], axis=0).T
        turned = jnp.concatenate([ow[i * 128 : (i + 1) * 128, :].T for i in range(groups)], axis=1)
        return gains, shifts, turned

    def project(buf, i, first, gains, shifts, turned):
        lanes = pl.ds(i * stride, stride)
        acc = jnp.zeros((128, stride), F32)
        for t in range(groups):
            acc = acc + buf[t * 128 : (t + 1) * 128, lanes].astype(F32)
        row_mean = jnp.sum(acc, axis=0, keepdims=True) * (1.0 / whole)
        acc = jnp.zeros((128, stride), F32)
        for t in range(groups):
            off = buf[t * 128 : (t + 1) * 128, lanes].astype(F32) - row_mean
            acc = acc + off * off
        row_var = jnp.sum(acc, axis=0, keepdims=True) * (1.0 / whole)
        scale = lax.rsqrt(row_var + 1e-05)
        for t in range(groups):
            v = (buf[t * 128 : (t + 1) * 128, lanes].astype(F32) - row_mean) * scale
            v = v * gains[:, t : t + 1] + shifts[:, t : t + 1]
            buf[t * 128 : (t + 1) * 128, lanes] = (v * jnp.tanh(v) + v).astype(BF16)
        mixed = dot(turned, buf[:, lanes])
        mixed_ref[pl.ds(first + i * stride, stride), :] = mixed.T.astype(BF16)

    def turn(a):
        eye = (iota((count, count), 0) == iota((count, count), 1)).astype(F32).astype(BF16)
        return lax.dot_general(eye, a, (((1,), (1,)), ((), ())), preferred_element_type=F32).astype(BF16)

    def prepare():
        share_hi = share.astype(BF16)
        share_lo = (share - share_hi.astype(F32)).astype(BF16)
        tables = [turn(a) for a in (place_b, share_hi, share_lo)]
        for columns, bits, first, out in ((FAR_ROWS, 4, 6, mix), (NEAR * NEAR_SEND, 5, -4, mixn)):
            widen = owners((NEP, columns), 1, bits, first)
            slot_at, hi_at, lo_at = [dot(a, widen) for a in tables]
            slot = jnp.bitwise_and(iota((count, columns), 1), (1 << bits) - 1).astype(F32)
            for c in range(out.shape[0] // 2):
                there = slot_at == slot + float(HALF * c)
                out[2 * c] = jnp.where(there, hi_at, 0.0).astype(BF16)
                out[2 * c + 1] = jnp.where(there, lo_at, 0.0).astype(BF16)

    def weigh(table, c, back, r):
        back.arrive()
        return dot(table[2 * c], r[...]) + dot(table[2 * c + 1], r[...])

    kept = {}

    def first_up():
        loads[10].wait()
        loads[11].wait()
        up(x0, h0)

    def first_down():
        loads[12].wait()
        return_first()

    def project_early():
        gathers[0].finish()
        kept[0] = project_ready()
        project(cg, 0, half, *kept[0])

    def project_late():
        gathers[1].finish()
        project(cg_late, 0, 0, *kept[0])

    def add(table, c, back, r):
        value = weigh(table, c, back, r)
        kept[1] = kept[1] + value if 1 in kept else value

    work = (
        conv_late,
        send_near,
        go0.arrive,
        compact,
        first_up,
        lambda: up(x1, h1),
        up_near,
        first_down,
        return_second,
        return_near,
        project_early,
        lambda: project(cg, 1, half, *kept[0]),
        project_late,
        lambda: project(cg_late, 1, 0, *kept[0]),
        prepare,
        lambda: add(mix, 0, back0, r0),
        lambda: add(mixn, 0, backn, rn),
        lambda: add(mix, 1, back1, r1),
    )
    for step in ORDER:
        if step < 900:
            gathers[step // 100].run(step % 100)
        else:
            work[step - 900]()
    routed_ref[...] = kept[1].astype(BF16)

    halo_copy.wait_send()
    for transfer in (go0, go1, gon, *gathers[2:], back0, back1, backn):
        transfer.finish()


def body(
    value_in,
    gate_in,
    conv_kernel,
    norm_gain,
    norm_shift,
    out_weight,
    expert_input,
    expert_gain,
    route_ids,
    route_weights,
    gate_weight,
    up_weight,
    down_weight,
):
    length, channels = value_in.shape
    count, width = expert_input.shape
    cols = width // NTP
    vmem = pl.BlockSpec(memory_space=pltpu.VMEM)
    hbm = pl.BlockSpec(memory_space=pltpu.HBM)
    mixed_out, routed_out = pl.pallas_call(
        kernel,
        out_shape=(
            pltpu.VMEM((length, out_weight.shape[1]), BF16),
            pltpu.VMEM((count, cols), BF16),
        ),
        in_specs=[hbm] * 13,
        out_specs=(vmem, vmem),
        scratch_shapes=[
            pltpu.VMEM((channels, length), BF16),
            pltpu.VMEM((channels, length), BF16),
            pltpu.VMEM(conv_kernel.shape, F32),
            pltpu.VMEM((NTP * channels // 128, 128), F32),
            pltpu.VMEM((NTP * channels // 128, 128), F32),
            pltpu.VMEM((count, width), BF16),
            pltpu.VMEM((NTP, cols), F32),
            pltpu.VMEM(route_ids.shape[::-1], jnp.int32),
            pltpu.VMEM(route_ids.shape[::-1], F32),
            pltpu.VMEM((channels, 128 + length), F32),
            pltpu.VMEM((128, 32), F32),
            pltpu.VMEM((32, 128), F32),
            pltpu.VMEM((channels, 128), BF16),
            pltpu.VMEM((channels, 128), BF16),
            pltpu.VMEM((NTP * channels, length // 2), BF16),
            pltpu.VMEM((NTP * channels, length // 2), BF16),
            pltpu.VMEM((FAR_ROWS, cols), BF16),
            pltpu.VMEM((FAR_ROWS, cols), BF16),
            pltpu.VMEM((NEAR * NEAR_SEND, width), BF16),
            pltpu.VMEM((FAR_ROWS, cols), BF16),
            pltpu.VMEM((NEAR * NEAR_SEND, width), BF16),
            pltpu.VMEM((NTP * FAR_ROWS, cols), BF16),
            pltpu.VMEM((NTP * LATE_ROWS, cols), BF16),
            pltpu.VMEM((NTP * FAR_ROWS, cols), BF16),
            pltpu.VMEM((NTP * LATE_ROWS, cols), BF16),
            pltpu.VMEM((NTP * NEAR_ROWS, cols), BF16),
            pltpu.VMEM((FAR_ROWS, cols), BF16),
            pltpu.VMEM((FAR_ROWS, cols), BF16),
            pltpu.VMEM((NEAR * NEAR_SEND, cols), BF16),
            pltpu.VMEM((FAR_ROWS, cols), BF16),
            pltpu.VMEM((FAR_ROWS, cols), BF16),
            pltpu.VMEM((NEAR * NEAR_SEND, cols), BF16),
            pltpu.VMEM((4, count, FAR_ROWS), BF16),
            pltpu.VMEM((2, count, NEAR * NEAR_SEND), BF16),
            pltpu.VMEM(out_weight.shape, BF16),
            pltpu.VMEM((width, 2 * cols), BF16),
            pltpu.VMEM((width, cols), BF16),
            pltpu.SemaphoreType.DMA((13,)),
            pltpu.SemaphoreType.DMA((7,)),
            pltpu.SemaphoreType.DMA((7 * 23,)),
            pltpu.SemaphoreType.DMA((6,)),
            pltpu.SemaphoreType.DMA((6,)),
            pltpu.SemaphoreType.DMA((2,)),
        ],
        compiler_params=pltpu.CompilerParams(
            collective_id=0, has_side_effects=True, vmem_limit_bytes=60 * 1024 * 1024
        ),
        name="whole",
    )(
        value_in.T,
        gate_in.T,
        conv_kernel,
        norm_gain.reshape(-1, 128),
        norm_shift.reshape(-1, 128),
        expert_input,
        expert_gain.reshape(NTP, cols),
        route_ids.T,
        route_weights.T,
        out_weight,
        gate_weight,
        up_weight,
        down_weight,
    )
    return (mixed_out, routed_out)


def solution(mesh):
    return jax.shard_map(
        body,
        mesh=mesh,
        in_specs=(
            P("ep", "tp"),
            P("ep", "tp"),
            P(None, "tp"),
            P(),
            P(),
            P(None, "tp"),
            P("ep", None),
            P(),
            P("ep", None),
            P("ep", None),
            P("ep", None, "tp"),
            P("ep", None, "tp"),
            P("ep", None, "tp"),
        ),
        out_specs=(P("ep", "tp"), P("ep", "tp")),
        check_vma=False,
    )
```

time: 95.5 us -> 87.4 us (0.915)
  the two profiles are of different devices: /device:TPU:4 before, /device:TPU:2 now
where the time goes in v4:
time: 87.4 us; the launch traced here: 87.3 us
  Pallas kernels  85.3 us (98%)
  local copies, waits for them, and re-layouts  1.32 us (2%)
    pallas_call x1, Pallas kernels, body(): pl.pallas_call(kernel, out_shape=(pltpu.VMEM((length, out_weight.shape[1]...  85.3 us

profile of v4, /device:TPU:2, one launch (start us, length us, event | category | flops | bytes accessed | tf_op | source)
XLA Modules:
  0.0 87.3 jit_solution(7393826986863905974)
XLA Ops:
  0.6 85.3 %whole.1 = (bf16[1024,128]{1,0:T(8,128)(2,1)S(1)}, bf16[192,128]{1,0:T(8,128)(2,1)S(1)}) custom-call(bf16[96,1024]{1,0:T(8,128)(2,1)} %bitcast.7, bf16[96,1024]{1,0:T(8,128)(2,1)} %bitcast.8, f32[31,96]{1,0:T(8,128)} %taps_hbm.1, f32[12,128]{1,0:T(8,128)} %bitcast.9, f32[12,128]{1,0:T(8,128)} %bitcast.10, bf16[192,2048]{1,0:T(8,128)(2,1)} %rows_hbm.1, ...), custom_call_target="tpu_custom_call" | custom-call | tf_op jit(solution)/shard_map/whole/pallas_call | solution.py:608
  85.9 0.7 copy.17
  86.6 0.6 copy.18

commit v5 on v4

--- a/solution.py
+++ b/solution.py
@@ -25,18 +25,11 @@
 OFFS = (0, -1, 1, 2)
 
 ORDER = (
-    0, 900, 10, 11, 12, 13, 20, 21, 28, 29, 2, 22, 23, 30, 31, 24,
-    25, 3, 32, 33, 902, 200, 901, 26, 27, 34, 35, 212, 213, 210, 211, 220,
-    221, 903, 300, 228, 229, 1, 910, 230, 231, 203, 911, 222, 223, 224, 225, 232,
-    233, 202, 310, 311, 312, 313, 328, 329, 320, 321, 234, 235, 226, 227, 302, 322,
-    323, 330, 331, 324, 325, 303, 332, 333, 914, 201, 904, 400, 326, 327, 334, 335,
-    410, 411, 412, 413, 906, 420, 421, 428, 429, 301, 905, 500, 402, 422, 423, 430,
-    431, 424, 425, 403, 432, 433, 510, 511, 512, 513, 600, 520, 521, 528, 529, 426,
-    427, 434, 435, 502, 522, 523, 530, 531, 524, 525, 503, 532, 533, 610, 611, 612,
-    613, 620, 621, 628, 629, 401, 907, 100, 526, 527, 534, 535, 602, 622, 623, 630,
-    631, 624, 625, 603, 632, 633, 110, 111, 112, 113, 120, 121, 128, 129, 501, 908,
-    626, 627, 634, 635, 102, 122, 123, 130, 131, 124, 125, 103, 132, 133, 601, 909,
-    126, 127, 134, 135, 915, 101, 912, 913, 916, 917,
+    0, 900, 10, 20, 2, 21, 22, 901, 902, 200, 23, 210, 903, 300, 220, 1,
+    910, 911, 202, 221, 222, 310, 320, 223, 302, 321, 322, 914, 201, 904, 400, 323,
+    906, 410, 420, 301, 905, 500, 402, 421, 422, 510, 600, 520, 423, 502, 521, 522,
+    610, 620, 401, 907, 523, 100, 602, 621, 622, 501, 908, 110, 120, 623, 102, 121,
+    122, 601, 909, 123, 915, 101, 912, 913, 916, 917,
 )
 
 
@@ -49,7 +42,7 @@
         self.buf, self.axis = buf, axis
         self.height = buf.shape[0] // NTP
         self.size = self.height if axis == 0 else buf.shape[1]
-        self.send_sem, self.recv_sem, self.base = send.at[number], recv, number * 23
+        self.send_sem, self.recv_sem, self.base = send.at[number], recv, number * 7
         unit = 16 if axis == 0 else 128
         whole = self.size // unit
         self.spans = {}
@@ -76,8 +69,8 @@
 
     def sem(self, h, phase, k, n):
         if phase == 0:
-            return self.recv_sem.at[self.base + h * 11 + min(n, 2)]
-        return self.recv_sem.at[self.base + (h * 11 + 3 + 2 * k + n if n < 2 else 22)]
+            return self.recv_sem.at[self.base + n // 2]
+        return self.recv_sem.at[self.base + (2 + k if n < 2 else 6)]
 
     def wait(self, place, sem):
         pltpu.make_async_remote_copy(
@@ -106,11 +99,10 @@
         self.push(h, phase, k, first, 0, None, 1)
         self.push(h, phase, k, first, 0, None, -1)
 
-    def relay(self, h, phase, k, n):
+    def pass_on(self, h, phase, k, n):
         off = (-1, 1)[n]
         first = OFFS[k] if phase else off
         second = off if phase else 0
-        self.wait(self.place(h, first, second, None), self.sem(h, phase, k, n))
         self.push(h, phase, k, first, second, n, -off)
 
     def start(self):
@@ -122,19 +114,24 @@
     def run(self, step):
         if step == 0:
             self.start()
-        elif step == 1:
-            self.wait(self.buf.at[pl.ds(0, 4 * self.height)], self.sem(0, 1, 0, 2))
-        elif step < 10:
-            h = step - 2
-            self.wait(self.place(h, 2, 0, None), self.sem(h, 0, 0, 2))
-            self.both(h, 1, 3, 2)
-        elif step < 20:
-            h, n = (step - 10) // 2, step % 2
-            self.relay(h, 0, 0, n)
-            self.both(h, 1, n + 1, OFFS[n + 1])
-        else:
-            h, k, n = (step - 20) // 8, (step - 20) % 8 // 2, step % 2
-            self.relay(h, 1, k, n)
+            return
+        shards = 4 if step == 1 else 1 if step == 2 else 2
+        phase = 0 if step in (2, 10) else 1
+        k = step - 20 if step >= 20 else 0
+        self.wait(self.buf.at[pl.ds(0, shards * self.height)], self.sem(0, phase, k, 2 if step < 10 else 0))
+        for h in (0, 1):
+            if step == 2:
+                self.both(h, 1, 3, 2)
+            elif step == 10:
+                for n in (0, 1):
+                    self.pass_on(h, 0, 0, n)
+            elif step >= 20:
+                for n in (0, 1):
+                    self.pass_on(h, 1, k, n)
+        if step == 10:
+            for n in (0, 1):
+                for h in (0, 1):
+                    self.both(h, 1, n + 1, OFFS[n + 1])
 
     def finish(self):
         place = self.buf.at[pl.ds(0, (NTP - 1) * self.height)]
@@ -653,7 +650,7 @@
             pltpu.VMEM((width, cols), BF16),
             pltpu.SemaphoreType.DMA((13,)),
             pltpu.SemaphoreType.DMA((7,)),
-            pltpu.SemaphoreType.DMA((7 * 23,)),
+            pltpu.SemaphoreType.DMA((7 * 7,)),
             pltpu.SemaphoreType.DMA((6,)),
             pltpu.SemaphoreType.DMA((6,)),
             pltpu.SemaphoreType.DMA((2,)),

time: 87.4 us -> 85.3 us (0.976)
  the two profiles are of different devices: /device:TPU:2 before, /device:TPU:1 now
where the time goes in v5:
time: 85.3 us; the launch traced here: 83.9 us
  Pallas kernels  81.9 us (96%)
  local copies, waits for them, and re-layouts  1.32 us (2%)
    pallas_call x1, Pallas kernels, body(): pl.pallas_call(kernel, out_shape=(pltpu.VMEM((length, out_weight.shape[1]...  81.9 us

profile of v5, /device:TPU:1, one launch (start us, length us, event | category | flops | bytes accessed | tf_op | source)
XLA Modules:
  0.0 83.9 jit_solution(15335925297951135421)
XLA Ops:
  0.6 81.9 %whole.1 = (bf16[1024,128]{1,0:T(8,128)(2,1)S(1)}, bf16[192,128]{1,0:T(8,128)(2,1)S(1)}) custom-call(bf16[96,1024]{1,0:T(8,128)(2,1)} %bitcast.7, bf16[96,1024]{1,0:T(8,128)(2,1)} %bitcast.8, f32[31,96]{1,0:T(8,128)} %taps_hbm.1, f32[12,128]{1,0:T(8,128)} %bitcast.9, f32[12,128]{1,0:T(8,128)} %bitcast.10, bf16[192,2048]{1,0:T(8,128)(2,1)} %rows_hbm.1, ...), custom_call_target="tpu_custom_call" | custom-call | tf_op jit(solution)/shard_map/whole/pallas_call | solution.py:605
  82.6 0.7 copy.17
  83.3 0.6 copy.18

commit v6 on v5

--- a/solution.py
+++ b/solution.py
@@ -281,6 +281,9 @@
     rn,
     mix,
     mixn,
+    grow,
+    pack_near,
+    grow_near,
     ow,
     wgu,
     wd,
@@ -457,20 +460,18 @@
         room = NEAR * NEAR_SEND
         act = [activate(near[i * room // 2 : (i + 1) * room // 2, :]) for i in range(2)]
         own = pl.ds(pl.multiple_of(tp * NEAR_ROWS, 16), NEAR_ROWS)
-        turn_in = moved((NEAR_ROWS, room), 0, SLOTS, NEAR_SEND)
-        hn[own, :] = dot(turn_in, jnp.concatenate(act, axis=0)).astype(BF16)
+        hn[own, :] = dot(pack_near[...], jnp.concatenate(act, axis=0)).astype(BF16)
 
     def return_first():
         y0[...] = down(h0)
         back0.start()
 
     def return_second():
-        y1[...] = dot(moved((FAR_ROWS, LATE_ROWS), 1, OTHER, HALF), down(h1)).astype(BF16)
+        y1[...] = dot(grow[...], down(h1)).astype(BF16)
         back1.start()
 
     def return_near():
-        turn_out = moved((NEAR * NEAR_SEND, NEAR_ROWS), 1, SLOTS, NEAR_SEND)
-        yn[...] = dot(turn_out, down(hn)).astype(BF16)
+        yn[...] = dot(grow_near[...], down(hn)).astype(BF16)
         backn.start()
 
     whole = NTP * channels
@@ -510,6 +511,9 @@
         return lax.dot_general(eye, a, (((1,), (1,)), ((), ())), preferred_element_type=F32).astype(BF16)
 
     def prepare():
+        grow[...] = moved(grow.shape, 1, OTHER, HALF)
+        pack_near[...] = moved(pack_near.shape, 0, SLOTS, NEAR_SEND)
+        grow_near[...] = moved(grow_near.shape, 1, SLOTS, NEAR_SEND)
         share_hi = share.astype(BF16)
         share_lo = (share - share_hi.astype(F32)).astype(BF16)
         tables = [turn(a) for a in (place_b, share_hi, share_lo)]
@@ -645,6 +649,9 @@
             pltpu.VMEM((NEAR * NEAR_SEND, cols), BF16),
             pltpu.VMEM((4, count, FAR_ROWS), BF16),
             pltpu.VMEM((2, count, NEAR * NEAR_SEND), BF16),
+            pltpu.VMEM((FAR_ROWS, LATE_ROWS), BF16),
+            pltpu.VMEM((NEAR_ROWS, NEAR * NEAR_SEND), BF16),
+            pltpu.VMEM((NEAR * NEAR_SEND, NEAR_ROWS), BF16),
             pltpu.VMEM(out_weight.shape, BF16),
             pltpu.VMEM((width, 2 * cols), BF16),
             pltpu.VMEM((width, cols), BF16),

time: 85.3 us -> 85.4 us (level)
  no operation moved by 1% of the time
where the time goes in v6:
time: 85.4 us; the launch traced here: 83.8 us
  Pallas kernels  81.9 us (96%)
  local copies, waits for them, and re-layouts  1.32 us (2%)
    pallas_call x1, Pallas kernels, body(): pl.pallas_call(kernel, out_shape=(pltpu.VMEM((length, out_weight.shape[1]...  81.9 us

profile of v6, /device:TPU:1, one launch (start us, length us, event | category | flops | bytes accessed | tf_op | source)
XLA Modules:
  0.0 83.8 jit_solution(7384797852096605810)
XLA Ops:
  0.6 81.9 %whole.1 = (bf16[1024,128]{1,0:T(8,128)(2,1)S(1)}, bf16[192,128]{1,0:T(8,128)(2,1)S(1)}) custom-call(bf16[96,1024]{1,0:T(8,128)(2,1)} %bitcast.7, bf16[96,1024]{1,0:T(8,128)(2,1)} %bitcast.8, f32[31,96]{1,0:T(8,128)} %taps_hbm.1, f32[12,128]{1,0:T(8,128)} %bitcast.9, f32[12,128]{1,0:T(8,128)} %bitcast.10, bf16[192,2048]{1,0:T(8,128)(2,1)} %rows_hbm.1, ...), custom_call_target="tpu_custom_call" | custom-call | tf_op jit(solution)/shard_map/whole/pallas_call | solution.py:609
  82.5 0.7 copy.17
  83.2 0.6 copy.18
